TPU v7x, 128 devices: a whole 4x4x4 slice. The times are simulated.
128 devices in a mesh: ep: 64 (over z, y, x), tp: 2 (over core).
Axes of the slice: x: 4, y: 4, z: 4, core: 2. Of those that a mesh axis runs over, the one named last changes fastest.
Arguments:
- tokens: bfloat16 [16384, 1024], P('ep'), may hold values from -6 to 6
- norm_gain: float32 [1024], replicated, may hold values from 0.1 to 1.9
- routing: int32 [16384, 2], P('ep'), may hold values from 0 to 127, all different within a row; in each aligned block of 256 rows (0 to 255, 256 to 511, ...) at most 4 rows name the same one
- route_weights: float32 [16384, 2], P('ep'), may hold values from 0.1 to 1
- lengths: int32 [4096], P('ep'), may hold values from 1 to 4, 10240 in all
- w_gate: bfloat16 [128, 1024, 3584], P('ep', None, 'tp'), may hold values from -0.1875 to 0.1875
- w_up: bfloat16 [128, 1024, 3584], P('ep', None, 'tp'), may hold values from -0.1875 to 0.1875
- w_down: bfloat16 [128, 3584, 1024], P('ep', 'tp'), may hold values from -0.09375 to 0.09375
Outputs:
- mixed: bfloat16 [16384, 1024], P('ep', 'tp')
Inputs may be any that keep to these rules, and one draw needn't show every extreme that they name: `routing`: each row names 2 different experts; at most 4 rows of one device name the same expert, and that many is reached.
All inputs are finite; a program needn't handle non-finite values. No bound on the sum of `lengths` on one device may be relied on, other than what follows from the above.
Results may differ from a plain program's by a relative error of at most 0.009.
Values may be sent and summed in bfloat16 or wider, within the bound.
No kernel may reach another device: no remote copies, remote signals or barrier semaphores. Data moves between devices by JAX's collectives and lax.ppermute only.
A program may use at most 64 MiB of HBM per device.

v0:
```python
import jax
import jax.numpy as jnp
from jax import lax
from jax.sharding import PartitionSpec as P

SPAN = 4


eps = 1e-06


def laid_out(pieces, dim):
    shape = list(pieces.shape[1:])
    shape[dim] *= pieces.shape[0]
    return jnp.moveaxis(pieces, 0, dim).reshape(shape)


def sent_to_all(x, axis):
    copies = jnp.broadcast_to(x, (lax.axis_size(axis), *x.shape))
    return lax.all_to_all(copies, axis, split_axis=0, concat_axis=0, tiled=True)


def collect(x, axis, dim):
    return laid_out(sent_to_all(x, axis), dim)


def split_up(x, dim, devices):
    shape = x.shape
    pieces = x.reshape(*shape[:dim], devices, shape[dim] // devices, *shape[dim + 1 :])
    return jnp.moveaxis(pieces, dim, 0)


def sent_and_summed(x, axis, dim):
    pieces = split_up(x, dim, lax.axis_size(axis))
    arrived = lax.all_to_all(pieces, axis, split_axis=0, concat_axis=0, tiled=True)
    return arrived.astype(jnp.float32).sum(axis=0)


def per_device(tokens, norm_gain, routing, route_weights, lengths, w_gate, w_up, w_down):
    ep_count = lax.axis_size("ep")
    local_experts = w_gate.shape[0]
    experts_all = ep_count * local_experts
    tok_rows = tokens.shape[0]
    model_width = tokens.shape[1]
    chosen = routing.shape[1]
    bound = 2 * ((tok_rows * chosen + 2 * experts_all - 1) // (2 * experts_all))
    slots_all = experts_all * bound
    floats = tokens.astype(jnp.float32)
    normed = (
        floats * lax.rsqrt(jnp.mean(floats * floats, axis=-1, keepdims=True) + eps) * norm_gain
    ).astype(jnp.bfloat16)
    position = jnp.arange(tok_rows, dtype=jnp.int32)
    live_rows = position % SPAN < jnp.repeat(lengths, SPAN)
    expert_ids = routing.reshape(-1)
    live_picks = jnp.repeat(live_rows, chosen)
    onehot = (
        (expert_ids[:, None] == jnp.arange(experts_all, dtype=jnp.int32)[None, :])
        & live_picks[:, None]
    ).astype(jnp.int32)
    before = jnp.cumsum(onehot, axis=0) - onehot
    slot_rank = jnp.sum(before * onehot, axis=1)
    slot_index = jnp.where(live_picks, expert_ids * bound + slot_rank, slots_all)
    picked = (slot_index[None, :] == jnp.arange(slots_all, dtype=jnp.int32)[:, None]).reshape(
        slots_all, tok_rows, chosen
    )
    placing = jnp.any(picked, axis=2).astype(jnp.bfloat16)
    outgoing = jnp.dot(placing, normed, preferred_element_type=jnp.float32).astype(jnp.bfloat16)
    outgoing = outgoing.reshape(ep_count, local_experts, bound, model_width)
    half_bound = bound // 2
    own_half = lax.dynamic_slice_in_dim(outgoing, lax.axis_index("tp") * half_bound, half_bound, 2)
    arrived = lax.all_to_all(own_half, "ep", split_axis=0, concat_axis=0, tiled=True)
    incoming = collect(arrived, "tp", 2)
    gate_proj = jnp.einsum("sxcd,xdf->sxcf", incoming, w_gate, preferred_element_type=jnp.float32)
    up_proj = jnp.einsum("sxcd,xdf->sxcf", incoming, w_up, preferred_element_type=jnp.float32)
    hidden = (jax.nn.silu(gate_proj) * up_proj).astype(jnp.bfloat16)
    partial_out = jnp.einsum("sxcf,xfd->sxcd", hidden, w_down, preferred_element_type=jnp.float32)
    expert_out = sent_and_summed(partial_out.astype(jnp.bfloat16), "tp", 3).astype(jnp.bfloat16)
    returned = lax.all_to_all(expert_out, "ep", split_axis=0, concat_axis=0, tiled=True)
    returned = returned.reshape(slots_all, returned.shape[3])
    combine = jnp.sum(jnp.where(picked, route_weights[None, :, :], 0.0), axis=2)
    mixed = jnp.einsum("st,sd->td", combine, returned.astype(jnp.float32))
    return mixed.astype(jnp.bfloat16)


def solution(mesh):
    placed = (
        P("ep", None),
        P(),
        P("ep", None),
        P("ep", None),
        P("ep"),
        P("ep", None, "tp"),
        P("ep", None, "tp"),
        P("ep", "tp", None),
    )
    return jax.shard_map(
        per_device, mesh=mesh, in_specs=placed, out_specs=P("ep", "tp"), check_vma=False
    )
```

profile of v0, /device:TPU:1, one launch (start us, length us, event | category | flops | bytes accessed | tf_op | source)
XLA Modules:
  0.0 76.9 jit_solution(17570593586073391496)
XLA Ops:
  0.0 0.8 %copy.82 = s32[256,2]{1,0:T(8,128)S(1)} copy(s32[256,2]{0,1:T(2,128)} %param.10) | data formatting | bytes 4096 | tf_op args[2]
  0.8 0.1 eq.45
  1.0 0.1 eq.41
  1.2 0.7 broadcast_in_dim.43
  2.3 0.2 broadcast_in_dim.47
  2.4 0.1 copy.86
  2.6 0.3 fusion.24
  3.0 0.7 broadcast_in_dim.41
  4.0 0.2 and.27
  4.1 0.3 fusion.23
  4.4 0.1 reduce_sum.42
  4.7 1.0 %add_select_fusion.1 = s32[256,2]{0,1:T(2,128)S(1)} fusion(s32[256,2]{0,1:T(2,128)S(1)} %copy.88, s32[256,2]{0,1:T(2,128)} %param.10, pred[256]{0:T(512)(128)(4,1)S(1)} %fusion.35), kind=kLoop, calls=%fused_computation.42 | loop fusion | flops 1536 | bytes 6400 | tf_op jit(solution)/shard_map/jit(_where)/select_n | solution.py:62
  5.6 0.2 fusion.18
  5.8 1.2 %fusion.15 = f32[256]{0:T(256)S(1)} fusion(bf16[256,1024]{1,0:T(8,128)(2,1)} %param.8), kind=kLoop, calls=%fused_computation.18 | loop fusion | flops 786176 | bytes 525312 | tf_op jit(solution)/shard_map/reduce_sum | solution.py:50
  7.1 2.6 %convolution_convert_fusion = bf16[512,1024]{1,0:T(8,128)(2,1)} fusion(pred[512,256]{1,0:T(8,128)(4,1)S(1)} %fusion.18, bf16[256,1024]{1,0:T(8,128)(2,1)} %param.8, f32[1024]{0:T(1024)} %param.9, f32[256]{0:T(256)S(1)} %add_rsqrt_fusion), kind=kOutput, calls=%fused_computation.14 | convolution fusion | flops 270008320 | bytes 1709056 | tf_op jit(solution)/shard_map/dot_general | solution.py:67
  9.7 2.3 %reshape.79 = bf16[64,2,4,1024]{3,2,1,0:T(4,128)(2,1)} reshape(bf16[512,1024]{1,0:T(8,128)(2,1)} %convolution_convert_fusion) | data formatting | bytes 2097152 | tf_op jit(solution)/shard_map/reshape | solution.py:68
  11.9 1.8 %constant_dynamic-slice_fusion = bf16[64,2,2,1024]{3,2,1,0:T(2,128)(2,1)S(1)} fusion(bf16[64,2,4,1024]{3,2,1,0:T(4,128)(2,1)} %reshape.79, s32[]{:T(128)S(6)} %select_n.29), kind=kLoop, calls=%fused_computation.50 | loop fusion | bytes 1048580 | tf_op jit(solution)/shard_map/dynamic_slice | solution.py:70
  13.7 24.2 %all_to_all.20 = bf16[64,2,2,1024]{3,2,1,0:T(2,128)(2,1)S(1)} all-to-all(bf16[64,2,2,1024]{3,2,1,0:T(2,128)(2,1)S(1)} %constant_dynamic-slice_fusion), channel_id=1, replica_groups=mesh['ep'=64,'tp'=2] {'ep'}, dimensions={0} | all-to-all | bytes 1048576 | tf_op jit(solution)/shard_map/all_to_all | solution.py:71
  37.9 0.2 copy.89
  38.2 6.3 %all_to_all.21 = bf16[2,64,2,2,1024]{4,1,3,2,0:T(8,128)(2,1)S(1)} all-to-all(bf16[2,64,2,2,1024]{4,1,3,2,0:T(8,128)(2,1)S(1)} %broadcast_in_dim.51), channel_id=1, replica_groups=mesh['ep'=64,'tp'=2] {'tp'}, dimensions={0} | all-to-all | bytes 2097152 | tf_op jit(solution)/shard_map/all_to_all | solution.py:20
  44.7 2.1 %fusion.4 = f32[2,64,4,1792]{3,1,2,0:T(8,128)S(1)} fusion(bf16[64,2,4,1024]{3,0,2,1:T(8,128)(2,1)S(1)} %bitcast.65, bf16[2,1024,1792]{2,1,0:T(8,128)(2,1)S(1)} %bitcast.68), kind=kOutput, calls=%fused_computation.4 | convolution fusion | flops 1879048192 | bytes 12058624 | tf_op jit(solution)/shard_map/sxcd,xdf->sxcf/dot_general | solution.py:73
  46.8 0.9 %slice-done.3 = s8[3145728]{0:T(1024)(128)(4,1)S(1)} async-done(((s8[7340032]{0:T(1024)(128)(4,1)}), s8[3145728]{0:T(1024)(128)(4,1)S(1)}, s32[]{:S(2)}) %slice-start.3) | async-done | bytes 3145752
  47.8 2.3 %fusion.6 = bf16[64,2,4,1792]{3,0,2,1:T(8,128)(2,1)S(1)} fusion(f32[2,64,4,1792]{3,1,2,0:T(8,128)S(1)} %fusion.4, bf16[64,2,4,1024]{3,0,2,1:T(8,128)(2,1)S(1)} %bitcast.66, bf16[2,1024,1792]{2,1,0:T(8,128)(2,1)S(1)} %bitcast.76), kind=kOutput, calls=%fused_computation.7 | convolution fusion | flops 1884553216 | bytes 13893632 | tf_op jit(solution)/shard_map/sxcd,xdf->sxcf/dot_general | solution.py:74
  50.1 2.1 %fusion.12 = bf16[2,64,4,1024]{3,1,2,0:T(8,128)(2,1)S(1)} fusion(bf16[64,2,4,1792]{3,0,2,1:T(8,128)(2,1)S(1)} %fusion.6, bf16[2,1792,1024]{2,1,0:T(8,128)(2,1)S(1)} %bitcast.78), kind=kOutput, calls=%fused_computation.13 | convolution fusion | flops 1879572480 | bytes 10223616 | tf_op jit(solution)/shard_map/sxcf,xfd->sxcd/dot_general | solution.py:76
  52.3 4.6 %all_to_all.22 = bf16[2,64,2,4,512]{4,1,3,2,0:T(8,128)(2,1)S(1)} all-to-all(bf16[2,64,2,4,512]{4,1,3,2,0:T(8,128)(2,1)S(1)} %bitcast.70), channel_id=1, replica_groups=mesh['ep'=64,'tp'=2] {'tp'}, dimensions={0} | all-to-all | bytes 2097152 | tf_op jit(solution)/shard_map/all_to_all | solution.py:35
  56.9 0.4 reduce_sum.45
  57.3 1.2 %copy.93 = bf16[64,2,4,512]{3,2,1,0:T(4,128)(2,1)} copy(bf16[64,2,4,512]{3,0,2,1:T(8,128)(2,1)S(1)} %reduce_sum.45) | data formatting | bytes 1048576 | tf_op jit(solution)/shard_map/reduce_sum | solution.py:36
  58.5 4.6 %all-to-all-start.3 = ((bf16[64,2,4,512]{3,2,1,0:T(4,128)(2,1)}), bf16[64,2,4,512]{3,2,1,0:T(4,128)(2,1)S(1)}, u32[]{:S(2)}, u32[]{:S(2)}) async-start(bf16[64,2,4,512]{3,2,1,0:T(4,128)(2,1)} %copy.93), calls=%async_computation.3 | async-start | bytes 1048576 | tf_op jit(solution)/shard_map/all_to_all | solution.py:78
  63.1 0.2 select_reduce_fusion
  63.3 12.4 %all-to-all-done.3 = bf16[64,2,4,512]{3,2,1,0:T(4,128)(2,1)S(1)} async-done(((bf16[64,2,4,512]{3,2,1,0:T(4,128)(2,1)}), bf16[64,2,4,512]{3,2,1,0:T(4,128)(2,1)S(1)}, u32[]{:S(2)}, u32[]{:S(2)}) %all-to-all-start.3) | async-done | bytes 524320 | tf_op jit(solution)/shard_map/all_to_all | solution.py:78
  75.8 0.1 reshape.82
  75.9 1.0 %fusion.36 = bf16[256,512]{1,0:T(8,128)(2,1)} fusion(bf16[512,256]{1,0:T(8,128)(2,1)S(1)} %select_reduce_fusion, bf16[512,512]{1,0:T(8,128)(2,1)S(1)} %reshape.82), kind=kOutput, calls=%fused_computation.51 | convolution fusion | flops 134217728 | bytes 1048576 | tf_op jit(solution)/shard_map/st,sd->td/dot_general | solution.py:81
  (35 shorter events, 1.2 us)
Async XLA Ops:
  4.1 40.5 %slice-start = ((s8[7340032]{0:T(1024)(128)(4,1)}), s8[3145728]{0:T(1024)(128)(4,1)S(1)}, s32[]{:S(2)}) async-start(s8[7340032]{0:T(1024)(128)(4,1)} %bitcast.67), calls=%async_computation.4 | async-start | bytes 6291456
  13.7 31.0 %slice-start.1 = ((s8[7340032]{0:T(1024)(128)(4,1)}), s8[4194304]{0:T(1024)(128)(4,1)S(1)}, s32[]{:S(2)}) async-start(s8[7340032]{0:T(1024)(128)(4,1)} %bitcast.67), calls=%async_computation.5 | async-start | bytes 8388608
  44.5 2.3 %slice-start.2 = ((s8[7340032]{0:T(1024)(128)(4,1)}), s8[4194304]{0:T(1024)(128)(4,1)S(1)}, s32[]{:S(2)}) async-start(s8[7340032]{0:T(1024)(128)(4,1)} %bitcast.75), calls=%async_computation.6 | async-start | bytes 8388608
  44.7 3.1 %slice-start.3 = ((s8[7340032]{0:T(1024)(128)(4,1)}), s8[3145728]{0:T(1024)(128)(4,1)S(1)}, s32[]{:S(2)}) async-start(s8[7340032]{0:T(1024)(128)(4,1)} %bitcast.75), calls=%async_computation.7 | async-start | bytes 6291456
  44.7 5.4 %slice-start.4 = ((s8[7340032]{0:T(1024)(128)(4,1)}), s8[4194304]{0:T(1024)(128)(4,1)S(1)}, s32[]{:S(2)}) async-start(s8[7340032]{0:T(1024)(128)(4,1)} %bitcast.77), calls=%async_computation.8 | async-start | bytes 8388608
  47.8 2.4 %slice-start.5 = ((s8[7340032]{0:T(1024)(128)(4,1)}), s8[3145728]{0:T(1024)(128)(4,1)S(1)}, s32[]{:S(2)}) async-start(s8[7340032]{0:T(1024)(128)(4,1)} %bitcast.77), calls=%async_computation.9 | async-start | bytes 6291456
  52.2 10.9 %copy-start = (f32[256,2]{0,1:T(2,128)S(1)}, f32[256,2]{0,1:T(2,128)}, u32[]{:S(2)}) copy-start(f32[256,2]{0,1:T(2,128)} %param.11) | copy-start | bytes 6148
  58.5 17.3 %all-to-all-start.3 = ((bf16[64,2,4,512]{3,2,1,0:T(4,128)(2,1)}), bf16[64,2,4,512]{3,2,1,0:T(4,128)(2,1)S(1)}, u32[]{:S(2)}, u32[]{:S(2)}) async-start(bf16[64,2,4,512]{3,2,1,0:T(4,128)(2,1)} %copy.93), calls=%async_computation.3 | async-start | bytes 1048576 | tf_op jit(solution)/shard_map/all_to_all | solution.py:78
where the time goes:
time: 77.6 us; the launch traced here: 76.9 us
  blocking collectives  35.1 us (45%)
  waiting for transfers between devices  12.4 us (16%)
  local copies, waits for them, and re-layouts  10.7 us (14%)
  matrix products  10.1 us (13%)
  starting transfers between devices  4.63 us (6%)
  other arithmetic  3.69 us (5%)
    all_to_all x1, blocking collectives, per_device(): lax.all_to_all(own_half, 'ep', split_axis=0, concat_axis=0, tiled=True)  24.2 us
    all_to_all x1, waiting for transfers between devices, per_device(): lax.all_to_all(expert_out, 'ep', split_axis=0, concat_axis=0, tiled=True)  12.4 us
    all_to_all x1, blocking collectives, sent_to_all(): return lax.all_to_all(copies, axis, split_axis=0, concat_axis=0, tiled=True)  6.35 us
    all_to_all x1, starting transfers between devices, per_device(): lax.all_to_all(expert_out, 'ep', split_axis=0, concat_axis=0, tiled=True)  4.63 us
    all_to_all x1, blocking collectives, sent_and_summed(): lax.all_to_all(pieces, axis, split_axis=0, concat_axis=0, tiled=True)  4.57 us
    dot_general x1, matrix products, per_device(): jnp.dot(placing, normed, preferred_element_type=jnp.float32)  2.59 us
    dot_general x1, matrix products, per_device(): jnp.einsum('sxcd,xdf->sxcf', incoming, w_up, preferred_element_type=jnp.f...  2.33 us
    reshape x1, local copies, waits for them, and re-layouts, per_device(): outgoing = outgoing.reshape(ep_count, local_experts, bound, model_width)  2.27 us
  transfers between devices with their start and end apart: 1, of which 1 were waited for; matrix products, arithmetic and copies ran while one was open for 0% of the time, Pallas kernels for 0%

commit v1 on v0

v1 whole, which is shorter than its diff:
```python
import jax
import jax.numpy as jnp
from jax import lax
from jax.experimental import pallas as pl
from jax.experimental.pallas import tpu as pltpu
from jax.sharding import PartitionSpec as P

SPAN = 4
SLOTS = 4
CHUNK = 256
eps = 1e-06
f32 = jnp.float32
bf16 = jnp.bfloat16


def dot(a, b):
    return jnp.dot(a, b, preferred_element_type=f32)


def iota(shape, dim):
    return lax.broadcasted_iota(jnp.int32, shape, dim)


def in_hbm(*arrays):
    return [pltpu.with_memory_space_constraint(x, pltpu.HBM) for x in arrays]


def slot_codes(routes, lengths, experts):
    rows = routes.shape[1]
    seqs = lengths.shape[1]
    spread = (iota((seqs, rows), 1) // SPAN == iota((seqs, rows), 0)).astype(bf16)
    spans = dot(jnp.broadcast_to(lengths.astype(bf16), (8, seqs)), spread)[0:1]
    live = (iota((1, rows), 1) % SPAN).astype(f32) < spans
    ids = iota((experts, rows), 0)
    hit = ((routes[0:1] == ids) | (routes[1:2] == ids)) & live
    earlier = (iota((rows, rows), 0) < iota((rows, rows), 1)).astype(bf16)
    before = dot(hit.astype(bf16), earlier)
    return jnp.where(hit, before, -1.0)


def fetch(pairs, sems):
    copies = [pltpu.make_async_copy(src, dst, sems.at[i]) for i, (src, dst) in enumerate(pairs)]
    for copy in copies:
        copy.start()
    return copies


def prep_kernel(
    tok_hbm, gain_hbm, route_hbm, len_hbm, wg_ref, wu_ref, wd_ref,
    out_ref, sg_ref, su_ref, sd_ref,
    tok_ref, gain_ref, route_ref, len_ref, small_sems, sems,
):
    me = lax.axis_index("tp")
    small = fetch(
        ((route_hbm, route_ref), (len_hbm, len_ref), (gain_hbm, gain_ref), (tok_hbm, tok_ref)), small_sems
    )
    copies = [
        pltpu.make_async_copy(w.at[1 - me], s, sems.at[i])
        for i, (w, s) in enumerate(((wg_ref, sg_ref), (wu_ref, su_ref), (wd_ref, sd_ref)))
    ]
    for copy in copies:
        copy.start()
    for copy in small[:2]:
        copy.wait()
    rows, width = tok_ref.shape
    half = width // 2
    slots = out_ref.shape[0]
    chips = slots // 8
    codes = slot_codes(route_ref[...], len_ref[...], 2 * chips).astype(bf16)
    at = iota((slots, 2 * chips), 0)
    mine = (iota((slots, 2 * chips), 1) == 2 * (at // 8) + me).astype(bf16)
    wide = dot(mine, codes)
    row = iota((slots, rows), 0)
    here = wide == (row % SLOTS).astype(f32)
    upper = (row // SLOTS) % 2 == 1
    place_low = jnp.where(here & ~upper, 1.0, 0.0).astype(bf16)
    place_high = jnp.where(here & upper, 1.0, 0.0).astype(bf16)
    for copy in small[2:]:
        copy.wait()
    floats = tok_ref[...].astype(f32)
    scale = lax.rsqrt(jnp.mean(floats * floats, axis=-1, keepdims=True) + eps)
    normed = (floats * scale * gain_ref[...]).astype(bf16)
    out_ref[...] = (dot(place_low, normed[:, :half]) + dot(place_high, normed[:, half:])).astype(bf16)
    for copy in copies:
        copy.wait()


def prep(tokens, gain, routes, lengths, w_gate, w_up, w_down):
    width = tokens.shape[1]
    hidden = w_gate.shape[2]
    chips = lax.axis_size("ep")
    vmem = pl.BlockSpec(memory_space=pltpu.VMEM)
    hbm = pl.BlockSpec(memory_space=pltpu.HBM)
    return pl.pallas_call(
        prep_kernel,
        name="prep",
        out_shape=(
            jax.ShapeDtypeStruct((8 * chips, width // 2), bf16),
            pltpu.VMEM((width, hidden), bf16),
            pltpu.VMEM((width, hidden), bf16),
            pltpu.VMEM((hidden, width), bf16),
        ),
        in_specs=[hbm] * 7,
        out_specs=(vmem,) * 4,
        scratch_shapes=[
            pltpu.VMEM(tokens.shape, bf16),
            pltpu.VMEM(gain.shape, f32),
            pltpu.VMEM(routes.shape, jnp.int32),
            pltpu.VMEM(lengths.shape, jnp.int32),
            pltpu.SemaphoreType.DMA((4,)),
            pltpu.SemaphoreType.DMA((3,)),
        ],
        compiler_params=pltpu.CompilerParams(vmem_limit_bytes=12 << 20),
    )(*in_hbm(tokens, gain, routes, lengths, w_gate, w_up, w_down))


def expert_kernel(in_ref, wg_ref, wu_ref, wd_ref, sg_ref, su_ref, sd_ref, out_ref, g_buf, u_buf, d_buf, x_buf, h_buf, sems):
    me = lax.axis_index("tp")
    width, hidden = g_buf.shape
    half = width // 2
    parts = hidden // CHUNK
    gate_up = []
    for i in range(parts):
        cols = pl.ds(i * CHUNK, CHUNK)
        gate_up.append(
            (
                pltpu.make_async_copy(wg_ref.at[me, :, cols], g_buf.at[:, cols], sems.at[0, i]),
                pltpu.make_async_copy(wu_ref.at[me, :, cols], u_buf.at[:, cols], sems.at[1, i]),
            )
        )
    down = pltpu.make_async_copy(wd_ref.at[me], d_buf, sems.at[2, 0])
    for pair in gate_up:
        for copy in pair:
            copy.start()
    down.start()
    pairs = in_ref.shape[0] // 16
    arrived = in_ref[...].astype(f32).reshape(pairs, 2, 8, half)
    even, odd = arrived[:, 0], arrived[:, 1]
    low = iota((pairs, 8, half), 1) < SLOTS
    first = jnp.where(low, even, pltpu.roll(odd, SLOTS, 1))
    second = jnp.where(low, pltpu.roll(even, SLOTS, 1), odd)
    x_buf[:, :half] = first.reshape(pairs * 8, half).astype(bf16)
    x_buf[:, half:] = second.reshape(pairs * 8, half).astype(bf16)

    def part(gate_ref, up_ref, i, base):
        cols = pl.ds(i * CHUNK, CHUNK)
        x = x_buf[...]
        gate = dot(x, gate_ref[:, cols])
        up = dot(x, up_ref[:, cols])
        h_buf[:, pl.ds(base + i * CHUNK, CHUNK)] = (gate / (1.0 + jnp.exp(-gate)) * up).astype(bf16)

    for i in range(parts):
        part(sg_ref, su_ref, i, 0)
    for i in range(parts):
        for copy in gate_up[i]:
            copy.wait()
        part(g_buf, u_buf, i, hidden)
    down.wait()
    low = iota((pairs, 8, CHUNK), 1) < SLOTS

    def column(i):
        cols = pl.ds(i * CHUNK, CHUNK)
        total = dot(h_buf[:, :hidden], sd_ref[:, cols]) + dot(h_buf[:, hidden:], d_buf[:, cols])
        return total.reshape(pairs, 8, CHUNK)

    for core in range(2):
        a, b = column(2 * core), column(2 * core + 1)
        out_ref[:, 0, core] = jnp.where(low, a, pltpu.roll(b, SLOTS, 1)).astype(bf16)
        out_ref[:, 1, core] = jnp.where(low, pltpu.roll(a, SLOTS, 1), b).astype(bf16)


def expert(arrived, w_gate, w_up, w_down, sg, su, sd):
    width, hidden = sg.shape
    rows = arrived.shape[0] // 2
    vmem = pl.BlockSpec(memory_space=pltpu.VMEM)
    hbm = pl.BlockSpec(memory_space=pltpu.HBM)
    return pl.pallas_call(
        expert_kernel,
        name="expert",
        out_shape=jax.ShapeDtypeStruct((rows // 8, 2, 2, 8, width // 4), bf16),
        in_specs=[vmem] + [hbm] * 3 + [vmem] * 3,
        out_specs=vmem,
        scratch_shapes=[
            pltpu.VMEM((width, hidden), bf16),
            pltpu.VMEM((width, hidden), bf16),
            pltpu.VMEM((hidden, width), bf16),
            pltpu.VMEM((rows, width), bf16),
            pltpu.VMEM((rows, 2 * hidden), bf16),
            pltpu.SemaphoreType.DMA((3, hidden // CHUNK)),
        ],
        compiler_params=pltpu.CompilerParams(vmem_limit_bytes=24 << 20),
    )(arrived, *in_hbm(w_gate, w_up, w_down), sg, su, sd)


def combine_kernel(in_ref, route_ref, len_ref, weight_ref, out_ref):
    slots, quarter = in_ref.shape
    rows = route_ref.shape[1]
    experts = slots // 8
    routes = route_ref[...]
    codes = slot_codes(routes, len_ref[...], experts).astype(bf16)
    ids = iota((experts, rows), 0)
    weights = jnp.where(
        routes[0:1] == ids, weight_ref[0:1], jnp.where(routes[1:2] == ids, weight_ref[1:2], 0.0)
    ).astype(bf16)
    owner = (iota((slots, experts), 0) // 8 == iota((slots, experts), 1)).astype(bf16)
    row = iota((slots, rows), 0)
    picked = jnp.where(dot(owner, codes) == (row % SLOTS).astype(f32), dot(owner, weights), 0.0)
    upper = (row // SLOTS) % 2 == 1
    for part in range(2):
        mix = jnp.where(upper if part else ~upper, picked, 0.0).astype(bf16)
        mixed = lax.dot_general(mix, in_ref[...], (((0,), (0,)), ((), ())), preferred_element_type=f32)
        out_ref[:, part * quarter : (part + 1) * quarter] = mixed.astype(bf16)


def combine(returned, routes, lengths, weights):
    vmem = pl.BlockSpec(memory_space=pltpu.VMEM)
    return pl.pallas_call(
        combine_kernel,
        name="combine",
        out_shape=jax.ShapeDtypeStruct((routes.shape[1], 2 * returned.shape[1]), bf16),
        in_specs=[vmem] * 4,
        out_specs=vmem,
        compiler_params=pltpu.CompilerParams(vmem_limit_bytes=12 << 20),
    )(returned, routes, lengths, weights)


def per_device(tokens, norm_gain, routing, route_weights, lengths, w_gate, w_up, w_down):
    chips = lax.axis_size("ep")
    width = tokens.shape[1]
    routes = routing.T
    weights = route_weights.T
    spans = lengths.reshape(1, -1)
    outgoing, *halves = prep(tokens, norm_gain.reshape(1, -1), routes, spans, w_gate, w_up, w_down)
    swapped = [lax.ppermute(half, "tp", [(0, 1), (1, 0)]) for half in halves]
    arrived = lax.all_to_all(outgoing.reshape(chips, 8, width // 2), "ep", split_axis=0, concat_axis=0, tiled=True)
    results = expert(arrived.reshape(chips * 8, width // 2), w_gate, w_up, w_down, *swapped)
    returned = lax.all_to_all(
        results.reshape(2 * chips, 8, width // 4), ("ep", "tp"), split_axis=0, concat_axis=0, tiled=True
    )
    return combine(returned.reshape(chips * 16, width // 4), routes, spans, weights)


def solution(mesh):
    placed = (
        P("ep", None),
        P(),
        P("ep", None),
        P("ep", None),
        P("ep"),
        P("ep", None, "tp"),
        P("ep", None, "tp"),
        P("ep", "tp", None),
    )
    return jax.shard_map(
        per_device, mesh=mesh, in_specs=placed, out_specs=P("ep", "tp"), check_vma=False
    )
```

time: 77.6 us -> 59.1 us (0.76)
  Pallas kernels: 0 us -> 14.8 us
  waiting for transfers between devices: 12.4 us -> 0.01 us
  local copies, waits for them, and re-layouts: 10.7 us -> 0.02 us
  matrix products: 10.1 us -> 0 us
  blocking collectives: 35.1 us -> 42.1 us
  other arithmetic: 3.69 us -> 0 us
  starting transfers between devices: 4.63 us -> 1.97 us
    pallas_call x0 -> x3, Pallas kernels: none -> 14.8 us  [the longest x1 8.57 us: expert(): pl.pallas_call(expert_kernel, name='expert', out_shape=jax.ShapeDtypeStru...]
    all_to_all x1 -> x0, waiting for transfers between devices: 12.4 us -> none  [per_device(): lax.all_to_all(expert_out, 'ep', split_axis=0, concat_axis=0, tiled=True)]
    dot_general x5 -> x0, matrix products: 10.1 us -> none  [the longest x1 2.59 us: per_device(): jnp.dot(placing, normed, preferred_element_type=jnp.float32)]
    all_to_all x3 -> x2, blocking collectives: 35.1 us -> 42.1 us  [the longest x1 23.8 us: per_device(): lax.all_to_all(outgoing.reshape(chips, 8, width // 2), 'ep', split_axis=0...]
    all_to_all x1 -> x0, starting transfers between devices: 4.63 us -> none  [per_device(): lax.all_to_all(expert_out, 'ep', split_axis=0, concat_axis=0, tiled=True)]
    reshape x4 -> x0, local copies, waits for them, and re-layouts: 2.62 us -> none  [the longest x1 2.27 us: per_device(): outgoing = outgoing.reshape(ep_count, local_experts, bound, model_width)]
    broadcast_in_dim x9 -> x0, local copies, waits for them, and re-layouts: 2.25 us -> none  [the longest x4 1.63 us: per_device(): live_rows = position % SPAN < jnp.repeat(lengths, SPAN)]
    reduce_sum x4 -> x0, other arithmetic: 2.11 us -> none  [the longest x1 1.22 us: per_device(): jnp.mean(floats * floats, axis=-1, keepdims=True) + eps]
  transfers between devices with their start and end apart: 1 -> 3, of which waited for: 1 -> 0; matrix products, arithmetic and copies ran while one was open for 0% -> 0% of each run, Pallas kernels for 0% -> 0%
where the time goes in v1:
time: 59.1 us; the launch traced here: 58.9 us
  blocking collectives  42.1 us (71%)
  Pallas kernels  14.8 us (25%)
  starting transfers between devices  1.97 us (3%)
    all_to_all x1, blocking collectives, per_device(): lax.all_to_all(outgoing.reshape(chips, 8, width // 2), 'ep', split_axis=0...  23.8 us
    all_to_all x1, blocking collectives, per_device(): lax.all_to_all(results.reshape(2 * chips, 8, width // 4), ('ep', 'tp'), s...  18.3 us
    pallas_call x1, Pallas kernels, expert(): pl.pallas_call(expert_kernel, name='expert', out_shape=jax.ShapeDtypeStru...  8.57 us
    pallas_call x1, Pallas kernels, prep(): pl.pallas_call(prep_kernel, name='prep', out_shape=(jax.ShapeDtypeStruct(...  4.47 us
    ppermute x3, starting transfers between devices, per_device(): swapped = [lax.ppermute(half, 'tp', [(0, 1), (1, 0)]) for half in halves]  1.97 us
    pallas_call x1, Pallas kernels, combine(): pl.pallas_call(combine_kernel, name='combine', out_shape=jax.ShapeDtypeSt...  1.75 us
  transfers between devices with their start and end apart: 3, of which 0 were waited for; matrix products, arithmetic and copies ran while one was open for 0% of the time, Pallas kernels for 0%

profile of v1, /device:TPU:1, one launch (start us, length us, event | category | flops | bytes accessed | tf_op | source)
XLA Modules:
  0.0 58.9 jit_solution(1447012394476682567)
XLA Ops:
  0.0 4.5 %prep.1 = (bf16[512,512]{1,0:T(8,128)(2,1)S(1)}, bf16[1024,1792]{1,0:T(8,128)(2,1)S(1)}, bf16[1024,1792]{1,0:T(8,128)(2,1)S(1)}, bf16[1792,1024]{1,0:T(8,128)(2,1)S(1)}) custom-call(bf16[256,1024]{1,0:T(8,128)(2,1)} %tok_hbm.1, f32[1,1024]{1,0:T(1,128)} %bitcast.17, s32[2,256]{1,0:T(2,128)} %bitcast.12, s32[1,64]{1,0:T(1,128)} %bitcast.15, ...), custom_call_target="tpu_custom_call" | custom-call | tf_op jit(solution)/shard_map/prep/pallas_call | solution.py:94
  4.5 1.5 %collective-permute-start = (bf16[1024,1792]{1,0:T(8,128)(2,1)S(1)}, bf16[1024,1792]{1,0:T(8,128)(2,1)S(1)}, u32[]{:S(2)}, u32[]{:S(2)}) collective-permute-start(bf16[1024,1792]{1,0:T(8,128)(2,1)S(1)} %get-tuple-element.10), channel_id=1, source_target_pairs={{0,1},{1,0},{2,3},{3,2},{4,5},{5,4},{6,7},{7,6},{8,9},{9,8},{10,11... | collective-permute-start | bytes 11010056 | tf_op jit(solution)/shard_map/ppermute | solution.py:234
  5.9 0.1 collective-permute-start.1
  6.0 0.4 collective-permute-start.2
  6.4 23.8 %all_to_all.10 = bf16[64,8,512]{2,1,0:T(8,128)(2,1)S(1)} all-to-all(bf16[64,8,512]{2,1,0:T(8,128)(2,1)S(1)} %bitcast.11), channel_id=1, replica_groups=mesh['ep'=64,'tp'=2] {'ep'}, dimensions={0} | all-to-all | bytes 1048576 | tf_op jit(solution)/shard_map/all_to_all | solution.py:235
  30.2 0.0 collective-permute-done.sg_ref
  30.2 0.0 collective-permute-done.1.su_ref
  30.2 0.0 collective-permute-done.2.sd_ref
  30.2 0.0 copy-start
  30.2 0.0 copy-start.1
  30.3 0.0 copy-start.2
  30.3 8.6 %expert.1 = bf16[32,2,2,8,256]{4,3,2,1,0:T(8,128)(2,1)S(1)} custom-call(bf16[512,512]{1,0:T(8,128)(2,1)S(1)} %bitcast.8, bf16[2,1024,1792]{2,1,0:T(8,128)(2,1)} %wg_ref.3, bf16[2,1024,1792]{2,1,0:T(8,128)(2,1)} %wu_ref.3, bf16[2,1792,1024]{2,1,0:T(8,128)(2,1)} %wd_ref.3, bf16[1024,1792]{1,0:T(8,128)(2,1)S(1)} %collective-permute-done.sg_ref, ...), custom_call_target="tpu_custom_call" | custom-call | tf_op jit(solution)/shard_map/expert/pallas_call | solution.py:177
  38.8 18.3 %all_to_all.11 = bf16[128,8,256]{2,1,0:T(8,128)(2,1)S(1)} all-to-all(bf16[128,8,256]{2,1,0:T(8,128)(2,1)S(1)} %bitcast.9), channel_id=1, replica_groups=mesh['ep'=64,'tp'=2] {'ep','tp'}, dimensions={0} | all-to-all | bytes 1048576 | tf_op jit(solution)/shard_map/all_to_all | solution.py:237
  57.2 0.0 copy-done
  57.2 0.0 copy-done.1
  57.2 0.0 copy-done.2
  57.2 1.8 %combine.1 = bf16[256,512]{1,0:T(8,128)(2,1)} custom-call(bf16[1024,256]{1,0:T(8,128)(2,1)S(1)} %bitcast.10, s32[2,256]{1,0:T(2,128)S(1)} %bitcast.13, s32[1,64]{1,0:T(1,128)S(1)} %bitcast.16, f32[2,256]{1,0:T(2,128)S(1)} %bitcast.14), custom_call_target="tpu_custom_call" | custom-call | tf_op jit(solution)/shard_map/combine/pallas_call | solution.py:217
Async XLA Ops:
  4.5 25.7 %collective-permute-start = (bf16[1024,1792]{1,0:T(8,128)(2,1)S(1)}, bf16[1024,1792]{1,0:T(8,128)(2,1)S(1)}, u32[]{:S(2)}, u32[]{:S(2)}) collective-permute-start(bf16[1024,1792]{1,0:T(8,128)(2,1)S(1)} %get-tuple-element.10), channel_id=1, source_target_pairs={{0,1},{1,0},{2,3},{3,2},{4,5},{5,4},{6,7},{7,6},{8,9},{9,8},{10,11... | collective-permute-start | bytes 11010056 | tf_op jit(solution)/shard_map/ppermute | solution.py:234
  5.9 24.3 %collective-permute-start.1 = (bf16[1024,1792]{1,0:T(8,128)(2,1)S(1)}, bf16[1024,1792]{1,0:T(8,128)(2,1)S(1)}, u32[]{:S(2)}, u32[]{:S(2)}) collective-permute-start(bf16[1024,1792]{1,0:T(8,128)(2,1)S(1)} %get-tuple-element.11), channel_id=1, source_target_pairs={{0,1},{1,0},{2,3},{3,2},{4,5},{5,4},{6,7},{7,6},{8,9},{9,8},{10,11... | collective-permute-start | bytes 11010056 | tf_op jit(solution)/shard_map/ppermute | solution.py:234
  6.0 24.2 %collective-permute-start.2 = (bf16[1792,1024]{1,0:T(8,128)(2,1)S(1)}, bf16[1792,1024]{1,0:T(8,128)(2,1)S(1)}, u32[]{:S(2)}, u32[]{:S(2)}) collective-permute-start(bf16[1792,1024]{1,0:T(8,128)(2,1)S(1)} %get-tuple-element.12), channel_id=1, source_target_pairs={{0,1},{1,0},{2,3},{3,2},{4,5},{5,4},{6,7},{7,6},{8,9},{9,8},{10,11... | collective-permute-start | bytes 11010056 | tf_op jit(solution)/shard_map/ppermute | solution.py:234
  30.2 26.9 %copy-start = (s32[256,2]{0,1:T(2,128)S(1)}, s32[256,2]{0,1:T(2,128)}, u32[]{:S(2)}) copy-start(s32[256,2]{0,1:T(2,128)} %param.10) | copy-start | bytes 6148
  30.2 26.9 %copy-start.1 = (f32[256,2]{0,1:T(2,128)S(1)}, f32[256,2]{0,1:T(2,128)}, u32[]{:S(2)}) copy-start(f32[256,2]{0,1:T(2,128)} %param.11) | copy-start | bytes 6148
  30.3 26.9 %copy-start.2 = (s32[64]{0:T(128)S(1)}, s32[64]{0:T(128)}, u32[]{:S(2)}) copy-start(s32[64]{0:T(128)} %param.12) | copy-start | bytes 772

commit v2 on v1

v2 whole, which is shorter than its diff:
```python
import jax
import jax.numpy as jnp
from jax import lax
from jax.experimental import pallas as pl
from jax.experimental.pallas import tpu as pltpu
from jax.sharding import PartitionSpec as P

SPAN = 4
SLOTS = 4
CHUNK = 256
eps = 1e-06
f32 = jnp.float32
bf16 = jnp.bfloat16


def dot(a, b):
    return jnp.dot(a, b, preferred_element_type=f32)


def turned(a, b):
    return lax.dot_general(a, b, (((0,), (0,)), ((), ())), preferred_element_type=f32)


def iota(shape, dim):
    return lax.broadcasted_iota(jnp.int32, shape, dim)


def in_hbm(*arrays):
    return [pltpu.with_memory_space_constraint(x, pltpu.HBM) for x in arrays]


def slot_codes(routes, lengths, experts):
    rows = routes.shape[1]
    seqs = lengths.shape[1]
    spread = (iota((seqs, rows), 1) // SPAN == iota((seqs, rows), 0)).astype(bf16)
    spans = dot(jnp.broadcast_to(lengths.astype(bf16), (8, seqs)), spread)[0:1]
    live = (iota((1, rows), 1) % SPAN).astype(f32) < spans
    ids = iota((experts, rows), 0)
    hit = ((routes[0:1] == ids) | (routes[1:2] == ids)) & live
    earlier = (iota((rows, rows), 0) < iota((rows, rows), 1)).astype(bf16)
    before = dot(hit.astype(bf16), earlier)
    return jnp.where(hit, before, -1.0)


def fetch(pairs, sems):
    copies = [pltpu.make_async_copy(src, dst, sems.at[i]) for i, (src, dst) in enumerate(pairs)]
    for copy in copies:
        copy.start()
    return copies


def prep_kernel(
    tok_hbm, gain_hbm, route_hbm, len_hbm, share_hbm, wg_ref, wu_ref, wd_ref,
    out_ref, mix_ref, sgu_ref, sd_ref,
    tok_ref, gain_ref, route_ref, len_ref, share_ref, small_sems, sems,
):
    me = lax.axis_index("tp")
    small = fetch(
        (
            (route_hbm, route_ref), (len_hbm, len_ref), (tok_hbm, tok_ref), (gain_hbm, gain_ref),
            (share_hbm, share_ref),
        ),
        small_sems,
    )
    large = fetch(
        ((wg_ref.at[1 - me], sgu_ref.at[0]), (wu_ref.at[1 - me], sgu_ref.at[1]), (wd_ref.at[1 - me], sd_ref)), sems
    )
    for copy in small[:2]:
        copy.wait()
    rows, width = tok_ref.shape
    half = width // 2
    slots = out_ref.shape[0]
    experts = slots // 4
    routes = route_ref[...]
    codes = slot_codes(routes, len_ref[...], experts).astype(bf16)
    at = iota((slots, experts), 0)
    mine = (iota((slots, experts), 1) == 2 * (at // 8) + me).astype(bf16)
    wide = dot(mine, codes)
    row = iota((slots, rows), 0)
    here = wide == (row % SLOTS).astype(f32)
    upper = (row // SLOTS) % 2 == 1
    place_low = jnp.where(here & ~upper, 1.0, 0.0).astype(bf16)
    place_high = jnp.where(here & upper, 1.0, 0.0).astype(bf16)
    for copy in small[2:]:
        copy.wait()
    floats = tok_ref[...].astype(f32)
    scale = lax.rsqrt(jnp.mean(floats * floats, axis=-1, keepdims=True) + eps)
    normed = (floats * scale * gain_ref[...]).astype(bf16)
    out_ref[...] = (dot(place_low, normed[:, :half]) + dot(place_high, normed[:, half:])).astype(bf16)
    ids = iota((experts, rows), 0)
    shares = jnp.where(
        routes[0:1] == ids, share_ref[0:1], jnp.where(routes[1:2] == ids, share_ref[1:2], 0.0)
    ).astype(bf16)
    owner = (iota((experts, 2 * slots), 0) == iota((experts, 2 * slots), 1) // 8).astype(bf16)
    column = iota((rows, 2 * slots), 1)
    chosen = turned(codes, owner) == (column % SLOTS).astype(f32)
    picked = jnp.where(chosen, turned(shares, owner), 0.0)
    upper = (column // SLOTS) % 2 == 1
    mix_ref[0] = jnp.where(upper, 0.0, picked).astype(bf16)
    mix_ref[1] = jnp.where(upper, picked, 0.0).astype(bf16)
    for copy in large:
        copy.wait()


def prep(tokens, gain, routes, lengths, shares, w_gate, w_up, w_down):
    rows, width = tokens.shape
    hidden = w_gate.shape[2]
    chips = lax.axis_size("ep")
    return pl.pallas_call(
        prep_kernel,
        name="prep",
        out_shape=(
            jax.ShapeDtypeStruct((8 * chips, width // 2), bf16),
            pltpu.VMEM((2, rows, 16 * chips), bf16),
            pltpu.VMEM((2, width, hidden), bf16),
            pltpu.VMEM((hidden, width), bf16),
        ),
        in_specs=[pl.BlockSpec(memory_space=pltpu.HBM)] * 8,
        out_specs=(pl.BlockSpec(memory_space=pltpu.VMEM),) * 4,
        scratch_shapes=[
            pltpu.VMEM(tokens.shape, bf16),
            pltpu.VMEM(gain.shape, f32),
            pltpu.VMEM(routes.shape, jnp.int32),
            pltpu.VMEM(lengths.shape, jnp.int32),
            pltpu.VMEM(shares.shape, f32),
            pltpu.SemaphoreType.DMA((5,)),
            pltpu.SemaphoreType.DMA((3,)),
        ],
        compiler_params=pltpu.CompilerParams(vmem_limit_bytes=12 << 20),
    )(*in_hbm(tokens, gain, routes, lengths, shares, w_gate, w_up, w_down))


def expert_kernel(
    in_ref, sgu_ref, sd_ref, wg_ref, wu_ref, wd_ref, out_ref,
    gu_buf, d_buf, x_buf, y_buf, h_buf, sum_buf, gu_sems, d_sems,
):
    me = lax.axis_index("tp")
    hidden, width = d_buf.shape
    half = width // 2
    parts = hidden // CHUNK
    blocks = width // CHUNK
    pieces = []
    for i in range(blocks):
        rows = pl.ds(i * CHUNK, CHUNK)
        pieces.append((wg_ref.at[me, rows], gu_buf.at[0, rows]))
        pieces.append((wu_ref.at[me, rows], gu_buf.at[1, rows]))
    gate_up = fetch(pieces, gu_sems)
    pairs = in_ref.shape[0] // 16
    slots = 8 * pairs
    arrived = in_ref[...].astype(f32).reshape(pairs, 2, 8, half)
    even, odd = arrived[:, 0], arrived[:, 1]
    low = iota((pairs, 8, half), 1) < SLOTS
    first = jnp.where(low, even, pltpu.roll(odd, SLOTS, 1)).reshape(slots, half)
    second = jnp.where(low, pltpu.roll(even, SLOTS, 1), odd).reshape(slots, half)
    peak = jnp.zeros((slots, 128), f32)
    for i in range(half // 128):
        lanes = slice(i * 128, (i + 1) * 128)
        peak = jnp.maximum(peak, jnp.maximum(jnp.abs(first[:, lanes]), jnp.abs(second[:, lanes])))
    filled = lax.dot_general(
        jnp.ones((8, 128), bf16), (peak > 0.0).astype(bf16), (((1,), (1,)), ((), ())), preferred_element_type=f32
    )
    live = filled > 0.0
    earlier = (iota((slots, slots), 0) < iota((slots, slots), 1)).astype(bf16)
    place = jnp.where(live, dot(live.astype(bf16), earlier), -1.0)
    amount = jnp.sum(live[0:1].astype(jnp.int32))
    squeeze = (iota((slots, slots), 0).astype(f32) == place[0:1]).astype(bf16)
    x_buf[:, :half] = dot(squeeze, first.astype(bf16)).astype(bf16)
    x_buf[:, half:] = dot(squeeze, second.astype(bf16)).astype(bf16)

    def hide(rows, weights):
        x = x_buf[:rows]
        for i in range(parts):
            cols = pl.ds(i * CHUNK, CHUNK)
            gate = dot(x, weights[0, :, cols])
            up = dot(x, weights[1, :, cols])
            h_buf[:rows, cols] = (gate / (1.0 + jnp.exp(-gate)) * up).astype(bf16)

    def run(rows):
        hide(rows, sgu_ref)
        down = fetch(
            [(wd_ref.at[me, pl.ds(i * CHUNK, CHUNK)], d_buf.at[pl.ds(i * CHUNK, CHUNK)]) for i in range(parts)], d_sems
        )
        for i in range(blocks):
            cols = pl.ds(i * CHUNK, CHUNK)
            sum_buf[:rows, cols] = dot(h_buf[:rows], sd_ref[:, cols])
        for copy in gate_up:
            copy.wait()
        hide(rows, gu_buf)
        for copy in down:
            copy.wait()
        for i in range(blocks):
            cols = pl.ds(i * CHUNK, CHUNK)
            y_buf[:rows, cols] = (sum_buf[:rows, cols] + dot(h_buf[:rows], d_buf[:, cols])).astype(bf16)
        if rows < slots:
            y_buf[rows:] = jnp.zeros((slots - rows, width), bf16)

    few = slots * 3 // 4

    @pl.when(amount <= few)
    def _():
        run(few)

    @pl.when(amount > few)
    def _():
        run(slots)

    low = iota((pairs, 8, CHUNK), 1) < SLOTS

    def spread(i):
        return turned(squeeze, y_buf[:, i * CHUNK : (i + 1) * CHUNK]).reshape(pairs, 8, CHUNK)

    for core in range(2):
        a, b = spread(2 * core), spread(2 * core + 1)
        out_ref[:, 0, core] = jnp.where(low, a, pltpu.roll(b, SLOTS, 1)).astype(bf16)
        out_ref[:, 1, core] = jnp.where(low, pltpu.roll(a, SLOTS, 1), b).astype(bf16)


def expert(arrived, gate_up, down, w_gate, w_up, w_down):
    hidden, width = down.shape
    rows = arrived.shape[0] // 2
    vmem = pl.BlockSpec(memory_space=pltpu.VMEM)
    hbm = pl.BlockSpec(memory_space=pltpu.HBM)
    return pl.pallas_call(
        expert_kernel,
        name="expert",
        out_shape=jax.ShapeDtypeStruct((rows // 8, 2, 2, 8, width // 4), bf16),
        in_specs=[vmem] * 3 + [hbm] * 3,
        out_specs=vmem,
        scratch_shapes=[
            pltpu.VMEM((2, width, hidden), bf16),
            pltpu.VMEM((hidden, width), bf16),
            pltpu.VMEM((rows, width), bf16),
            pltpu.VMEM((rows, width), bf16),
            pltpu.VMEM((rows, hidden), bf16),
            pltpu.VMEM((rows, width), f32),
            pltpu.SemaphoreType.DMA((2 * (width // CHUNK),)),
            pltpu.SemaphoreType.DMA((hidden // CHUNK,)),
        ],
        compiler_params=pltpu.CompilerParams(vmem_limit_bytes=26 << 20),
    )(arrived, gate_up, down, *in_hbm(w_gate, w_up, w_down))


def combine_kernel(in_ref, mix_ref, out_ref):
    quarter = in_ref.shape[1]
    for part in range(2):
        out_ref[:, part * quarter : (part + 1) * quarter] = dot(mix_ref[part], in_ref[...]).astype(bf16)


def combine(returned, mix):
    vmem = pl.BlockSpec(memory_space=pltpu.VMEM)
    return pl.pallas_call(
        combine_kernel,
        name="combine",
        out_shape=jax.ShapeDtypeStruct((mix.shape[1], 2 * returned.shape[1]), bf16),
        in_specs=[vmem] * 2,
        out_specs=vmem,
        compiler_params=pltpu.CompilerParams(vmem_limit_bytes=8 << 20),
    )(returned, mix)


def per_device(tokens, norm_gain, routing, route_weights, lengths, w_gate, w_up, w_down):
    chips = lax.axis_size("ep")
    width = tokens.shape[1]
    routes = routing.T
    weights = route_weights.T
    spans = lengths.reshape(1, -1)
    outgoing, mix, gate_up, down = prep(
        tokens, norm_gain.reshape(1, -1), routes, spans, weights, w_gate, w_up, w_down
    )
    gate_up, down = (lax.ppermute(half, "tp", [(0, 1), (1, 0)]) for half in (gate_up, down))
    arrived = lax.all_to_all(outgoing.reshape(chips, 8, width // 2), "ep", split_axis=0, concat_axis=0, tiled=True)
    results = expert(arrived.reshape(chips * 8, width // 2), gate_up, down, w_gate, w_up, w_down)
    returned = lax.all_to_all(
        results.reshape(2 * chips, 8, width // 4), ("ep", "tp"), split_axis=0, concat_axis=0, tiled=True
    )
    return combine(returned.reshape(chips * 16, width // 4), mix)


def solution(mesh):
    placed = (
        P("ep", None),
        P(),
        P("ep", None),
        P("ep", None),
        P("ep"),
        P("ep", None, "tp"),
        P("ep", None, "tp"),
        P("ep", "tp", None),
    )
    return jax.shard_map(
        per_device, mesh=mesh, in_specs=placed, out_specs=P("ep", "tp"), check_vma=False
    )
```

time: 59.1 us -> 55.5 us (0.939)
  Pallas kernels: 14.8 us -> 11.7 us
    pallas_call x1, Pallas kernels: 8.57 us -> 6.1 us  [expert(): pl.pallas_call(expert_kernel, name='expert', out_shape=jax.ShapeDtypeStru...]
    pallas_call x1, Pallas kernels: 1.75 us -> 1.14 us  [combine(): pl.pallas_call(combine_kernel, name='combine', out_shape=jax.ShapeDtypeSt...]
    ppermute x3 -> x2, starting transfers between devices: 1.97 us -> 1.55 us  [per_device(): lax.ppermute(half, 'tp', [(0, 1), (1, 0)])]
  transfers between devices with their start and end apart: 3 -> 2, of which waited for: 0 -> 0; matrix products, arithmetic and copies ran while one was open for 0% -> 0% of each run, Pallas kernels for 0% -> 0%
where the time goes in v2:
time: 55.5 us; the launch traced here: 55.4 us
  blocking collectives  42.1 us (76%)
  Pallas kernels  11.7 us (21%)
  starting transfers between devices  1.55 us (3%)
    all_to_all x1, blocking collectives, per_device(): lax.all_to_all(outgoing.reshape(chips, 8, width // 2), 'ep', split_axis=0...  23.4 us
    all_to_all x1, blocking collectives, per_device(): lax.all_to_all(results.reshape(2 * chips, 8, width // 4), ('ep', 'tp'), s...  18.6 us
    pallas_call x1, Pallas kernels, expert(): pl.pallas_call(expert_kernel, name='expert', out_shape=jax.ShapeDtypeStru...  6.1 us
    pallas_call x1, Pallas kernels, prep(): pl.pallas_call(prep_kernel, name='prep', out_shape=(jax.ShapeDtypeStruct(...  4.5 us
    ppermute x2, starting transfers between devices, per_device(): lax.ppermute(half, 'tp', [(0, 1), (1, 0)])  1.55 us
    pallas_call x1, Pallas kernels, combine(): pl.pallas_call(combine_kernel, name='combine', out_shape=jax.ShapeDtypeSt...  1.14 us
  transfers between devices with their start and end apart: 2, of which 0 were waited for; matrix products, arithmetic and copies ran while one was open for 0% of the time, Pallas kernels for 0%

profile of v2, /device:TPU:1, one launch (start us, length us, event | category | flops | bytes accessed | tf_op | source)
XLA Modules:
  0.0 55.4 jit_solution(8785336689859631838)
XLA Ops:
  0.0 4.5 %prep.1 = (bf16[512,512]{1,0:T(8,128)(2,1)S(1)}, bf16[2,256,1024]{2,1,0:T(8,128)(2,1)S(1)}, bf16[2,1024,1792]{2,1,0:T(8,128)(2,1)S(1)}, bf16[1792,1024]{1,0:T(8,128)(2,1)S(1)}) custom-call(bf16[256,1024]{1,0:T(8,128)(2,1)} %tok_hbm.1, f32[1,1024]{1,0:T(1,128)} %bitcast.12, s32[2,256]{1,0:T(2,128)} %bitcast.13, s32[1,64]{1,0:T(1,128)} %bitcast.15, ...), custom_call_target="tpu_custom_call" | custom-call | tf_op jit(solution)/shard_map/prep/pallas_call | solution.py:109
  4.5 1.5 %collective-permute-start = (bf16[2,1024,1792]{2,1,0:T(8,128)(2,1)S(1)}, bf16[2,1024,1792]{2,1,0:T(8,128)(2,1)S(1)}, u32[]{:S(2)}, u32[]{:S(2)}) collective-permute-start(bf16[2,1024,1792]{2,1,0:T(8,128)(2,1)S(1)} %get-tuple-element.10), channel_id=1, source_target_pairs={{0,1},{1,0},{2,3},{3,2},{4,5},{5,4},{6,7},{7,6},{8,9},{9,8},{10,11... | collective-permute-start | bytes 22020104 | tf_op jit(solution)/shard_map/ppermute | solution.py:270
  6.0 0.1 collective-permute-start.1
  6.1 23.4 %all_to_all.10 = bf16[64,8,512]{2,1,0:T(8,128)(2,1)S(1)} all-to-all(bf16[64,8,512]{2,1,0:T(8,128)(2,1)S(1)} %bitcast.11), channel_id=1, replica_groups=mesh['ep'=64,'tp'=2] {'ep'}, dimensions={0} | all-to-all | bytes 1048576 | tf_op jit(solution)/shard_map/all_to_all | solution.py:271
  29.5 0.0 collective-permute-done.1.sd_ref
  29.5 0.0 collective-permute-done.sgu_ref
  29.5 6.1 %expert.1 = bf16[32,2,2,8,256]{4,3,2,1,0:T(8,128)(2,1)S(1)} custom-call(bf16[512,512]{1,0:T(8,128)(2,1)S(1)} %bitcast.8, bf16[2,1024,1792]{2,1,0:T(8,128)(2,1)S(1)} %collective-permute-done.sgu_ref, bf16[1792,1024]{1,0:T(8,128)(2,1)S(1)} %collective-permute-done.1.sd_ref, bf16[2,1024,1792]{2,1,0:T(8,128)(2,1)} %wg_ref.3, bf16[2,1024,1792]{2,1,0:T(8,128)(2,1)} %wu_ref.3, ...), custom_call_target="tpu_custom_call" | custom-call | tf_op jit(solution)/shard_map/expert/pallas_call | solution.py:223
  35.6 18.6 %all_to_all.11 = bf16[128,8,256]{2,1,0:T(8,128)(2,1)S(1)} all-to-all(bf16[128,8,256]{2,1,0:T(8,128)(2,1)S(1)} %bitcast.9), channel_id=1, replica_groups=mesh['ep'=64,'tp'=2] {'ep','tp'}, dimensions={0} | all-to-all | bytes 1048576 | tf_op jit(solution)/shard_map/all_to_all | solution.py:273
  54.2 1.1 %combine.1 = bf16[256,512]{1,0:T(8,128)(2,1)} custom-call(bf16[1024,256]{1,0:T(8,128)(2,1)S(1)} %bitcast.10, bf16[2,256,1024]{2,1,0:T(8,128)(2,1)S(1)} %get-tuple-element.12.mix_ref), custom_call_target="tpu_custom_call" | custom-call | tf_op jit(solution)/shard_map/combine/pallas_call | solution.py:251
Async XLA Ops:
  4.5 25.0 %collective-permute-start = (bf16[2,1024,1792]{2,1,0:T(8,128)(2,1)S(1)}, bf16[2,1024,1792]{2,1,0:T(8,128)(2,1)S(1)}, u32[]{:S(2)}, u32[]{:S(2)}) collective-permute-start(bf16[2,1024,1792]{2,1,0:T(8,128)(2,1)S(1)} %get-tuple-element.10), channel_id=1, source_target_pairs={{0,1},{1,0},{2,3},{3,2},{4,5},{5,4},{6,7},{7,6},{8,9},{9,8},{10,11... | collective-permute-start | bytes 22020104 | tf_op jit(solution)/shard_map/ppermute | solution.py:270
  6.0 23.5 %collective-permute-start.1 = (bf16[1792,1024]{1,0:T(8,128)(2,1)S(1)}, bf16[1792,1024]{1,0:T(8,128)(2,1)S(1)}, u32[]{:S(2)}, u32[]{:S(2)}) collective-permute-start(bf16[1792,1024]{1,0:T(8,128)(2,1)S(1)} %get-tuple-element.11), channel_id=1, source_target_pairs={{0,1},{1,0},{2,3},{3,2},{4,5},{5,4},{6,7},{7,6},{8,9},{9,8},{10,11... | collective-permute-start | bytes 11010056 | tf_op jit(solution)/shard_map/ppermute | solution.py:270

commit v3 on v2

--- a/solution.py
+++ b/solution.py
@@ -130,21 +130,12 @@
     )(*in_hbm(tokens, gain, routes, lengths, shares, w_gate, w_up, w_down))
 
 
-def expert_kernel(
-    in_ref, sgu_ref, sd_ref, wg_ref, wu_ref, wd_ref, out_ref,
-    gu_buf, d_buf, x_buf, y_buf, h_buf, sum_buf, gu_sems, d_sems,
-):
+def expert_kernel(in_ref, sgu_ref, sd_ref, wg_ref, wu_ref, wd_ref, out_ref, x_buf, y_buf, h_buf):
     me = lax.axis_index("tp")
-    hidden, width = d_buf.shape
+    hidden, width = sd_ref.shape
     half = width // 2
     parts = hidden // CHUNK
     blocks = width // CHUNK
-    pieces = []
-    for i in range(blocks):
-        rows = pl.ds(i * CHUNK, CHUNK)
-        pieces.append((wg_ref.at[me, rows], gu_buf.at[0, rows]))
-        pieces.append((wu_ref.at[me, rows], gu_buf.at[1, rows]))
-    gate_up = fetch(pieces, gu_sems)
     pairs = in_ref.shape[0] // 16
     slots = 8 * pairs
     arrived = in_ref[...].astype(f32).reshape(pairs, 2, 8, half)
@@ -167,30 +158,21 @@
     x_buf[:, :half] = dot(squeeze, first.astype(bf16)).astype(bf16)
     x_buf[:, half:] = dot(squeeze, second.astype(bf16)).astype(bf16)
 
-    def hide(rows, weights):
+    def hide(rows, gates, ups, base):
         x = x_buf[:rows]
         for i in range(parts):
             cols = pl.ds(i * CHUNK, CHUNK)
-            gate = dot(x, weights[0, :, cols])
-            up = dot(x, weights[1, :, cols])
-            h_buf[:rows, cols] = (gate / (1.0 + jnp.exp(-gate)) * up).astype(bf16)
+            gate = dot(x, gates[:, cols])
+            up = dot(x, ups[:, cols])
+            h_buf[:rows, pl.ds(base + i * CHUNK, CHUNK)] = (gate / (1.0 + jnp.exp(-gate)) * up).astype(bf16)
 
     def run(rows):
-        hide(rows, sgu_ref)
-        down = fetch(
-            [(wd_ref.at[me, pl.ds(i * CHUNK, CHUNK)], d_buf.at[pl.ds(i * CHUNK, CHUNK)]) for i in range(parts)], d_sems
-        )
+        hide(rows, sgu_ref.at[0], sgu_ref.at[1], 0)
+        hide(rows, wg_ref.at[me], wu_ref.at[me], hidden)
         for i in range(blocks):
             cols = pl.ds(i * CHUNK, CHUNK)
-            sum_buf[:rows, cols] = dot(h_buf[:rows], sd_ref[:, cols])
-        for copy in gate_up:
-            copy.wait()
-        hide(rows, gu_buf)
-        for copy in down:
-            copy.wait()
-        for i in range(blocks):
-            cols = pl.ds(i * CHUNK, CHUNK)
-            y_buf[:rows, cols] = (sum_buf[:rows, cols] + dot(h_buf[:rows], d_buf[:, cols])).astype(bf16)
+            total = dot(h_buf[:rows, :hidden], sd_ref[:, cols]) + dot(h_buf[:rows, hidden:], wd_ref[me, :, cols])
+            y_buf[:rows, cols] = total.astype(bf16)
         if rows < slots:
             y_buf[rows:] = jnp.zeros((slots - rows, width), bf16)
 
@@ -219,25 +201,19 @@
     hidden, width = down.shape
     rows = arrived.shape[0] // 2
     vmem = pl.BlockSpec(memory_space=pltpu.VMEM)
-    hbm = pl.BlockSpec(memory_space=pltpu.HBM)
     return pl.pallas_call(
         expert_kernel,
         name="expert",
         out_shape=jax.ShapeDtypeStruct((rows // 8, 2, 2, 8, width // 4), bf16),
-        in_specs=[vmem] * 3 + [hbm] * 3,
+        in_specs=[vmem] * 6,
         out_specs=vmem,
         scratch_shapes=[
-            pltpu.VMEM((2, width, hidden), bf16),
-            pltpu.VMEM((hidden, width), bf16),
             pltpu.VMEM((rows, width), bf16),
             pltpu.VMEM((rows, width), bf16),
-            pltpu.VMEM((rows, hidden), bf16),
-            pltpu.VMEM((rows, width), f32),
-            pltpu.SemaphoreType.DMA((2 * (width // CHUNK),)),
-            pltpu.SemaphoreType.DMA((hidden // CHUNK,)),
+            pltpu.VMEM((rows, 2 * hidden), bf16),
         ],
-        compiler_params=pltpu.CompilerParams(vmem_limit_bytes=26 << 20),
-    )(arrived, gate_up, down, *in_hbm(w_gate, w_up, w_down))
+        compiler_params=pltpu.CompilerParams(vmem_limit_bytes=8 << 20),
+    )(arrived, gate_up, down, *[pltpu.with_memory_space_constraint(w, pltpu.VMEM) for w in (w_gate, w_up, w_down)])
 
 
 def combine_kernel(in_ref, mix_ref, out_ref):

time: 55.5 us -> 55.3 us (level)
    pallas_call x1, Pallas kernels: 6.1 us -> 5.49 us  [expert(): pl.pallas_call(expert_kernel, name='expert', out_shape=jax.ShapeDtypeStru...]
where the time goes in v3:
time: 55.3 us; the launch traced here: 55.2 us
  blocking collectives  42.3 us (76%)
  Pallas kernels  11.3 us (20%)
  starting transfers between devices  1.55 us (3%)
    all_to_all x1, blocking collectives, per_device(): lax.all_to_all(outgoing.reshape(chips, 8, width // 2), 'ep', split_axis=0...  23.7 us
    all_to_all x1, blocking collectives, per_device(): lax.all_to_all(results.reshape(2 * chips, 8, width // 4), ('ep', 'tp'), s...  18.6 us
    pallas_call x1, Pallas kernels, expert(): pl.pallas_call(expert_kernel, name='expert', out_shape=jax.ShapeDtypeStru...  5.49 us
    pallas_call x1, Pallas kernels, prep(): pl.pallas_call(prep_kernel, name='prep', out_shape=(jax.ShapeDtypeStruct(...  4.63 us
    ppermute x2, starting transfers between devices, per_device(): lax.ppermute(half, 'tp', [(0, 1), (1, 0)])  1.55 us
    pallas_call x1, Pallas kernels, combine(): pl.pallas_call(combine_kernel, name='combine', out_shape=jax.ShapeDtypeSt...  1.14 us
  transfers between devices with their start and end apart: 2, of which 0 were waited for; matrix products, arithmetic and copies ran while one was open for 0% of the time, Pallas kernels for 0%

profile of v3, /device:TPU:1, one launch (start us, length us, event | category | flops | bytes accessed | tf_op | source)
XLA Modules:
  0.0 55.2 jit_solution(13801381061372475017)
XLA Ops:
  0.0 0.0 copy-start
  0.0 0.0 copy-start.1
  0.0 0.0 copy-start.2
  0.0 4.6 %prep.1 = (bf16[512,512]{1,0:T(8,128)(2,1)S(1)}, bf16[2,256,1024]{2,1,0:T(8,128)(2,1)S(1)}, bf16[2,1024,1792]{2,1,0:T(8,128)(2,1)S(1)}, bf16[1792,1024]{1,0:T(8,128)(2,1)S(1)}) custom-call(bf16[256,1024]{1,0:T(8,128)(2,1)} %tok_hbm.1, f32[1,1024]{1,0:T(1,128)} %bitcast.12, s32[2,256]{1,0:T(2,128)} %bitcast.13, s32[1,64]{1,0:T(1,128)} %bitcast.15, ...), custom_call_target="tpu_custom_call" | custom-call | tf_op jit(solution)/shard_map/prep/pallas_call | solution.py:109
  4.6 1.5 %collective-permute-start = (bf16[2,1024,1792]{2,1,0:T(8,128)(2,1)S(1)}, bf16[2,1024,1792]{2,1,0:T(8,128)(2,1)S(1)}, u32[]{:S(2)}, u32[]{:S(2)}) collective-permute-start(bf16[2,1024,1792]{2,1,0:T(8,128)(2,1)S(1)} %get-tuple-element.10), channel_id=1, source_target_pairs={{0,1},{1,0},{2,3},{3,2},{4,5},{5,4},{6,7},{7,6},{8,9},{9,8},{10,11... | collective-permute-start | bytes 22020104 | tf_op jit(solution)/shard_map/ppermute | solution.py:246
  6.1 0.1 collective-permute-start.1
  6.2 23.7 %all_to_all.10 = bf16[64,8,512]{2,1,0:T(8,128)(2,1)S(1)} all-to-all(bf16[64,8,512]{2,1,0:T(8,128)(2,1)S(1)} %bitcast.11), channel_id=1, replica_groups=mesh['ep'=64,'tp'=2] {'ep'}, dimensions={0} | all-to-all | bytes 1048576 | tf_op jit(solution)/shard_map/all_to_all | solution.py:247
  29.9 0.0 collective-permute-done.1.sd_ref
  29.9 0.0 collective-permute-done.sgu_ref
  29.9 0.0 copy-done
  29.9 0.0 copy-done.1
  29.9 0.0 copy-done.2
  29.9 5.5 %expert.1 = bf16[32,2,2,8,256]{4,3,2,1,0:T(8,128)(2,1)S(1)} custom-call(bf16[512,512]{1,0:T(8,128)(2,1)S(1)} %bitcast.8, bf16[2,1024,1792]{2,1,0:T(8,128)(2,1)S(1)} %collective-permute-done.sgu_ref, bf16[1792,1024]{1,0:T(8,128)(2,1)S(1)} %collective-permute-done.1.sd_ref, bf16[2,1024,1792]{2,1,0:T(8,128)(2,1)S(1)} %copy-done, ...), custom_call_target="tpu_custom_call" | custom-call | tf_op jit(solution)/shard_map/expert/pallas_call | solution.py:204
  35.4 18.6 %all_to_all.11 = bf16[128,8,256]{2,1,0:T(8,128)(2,1)S(1)} all-to-all(bf16[128,8,256]{2,1,0:T(8,128)(2,1)S(1)} %bitcast.9), channel_id=1, replica_groups=mesh['ep'=64,'tp'=2] {'ep','tp'}, dimensions={0} | all-to-all | bytes 1048576 | tf_op jit(solution)/shard_map/all_to_all | solution.py:249
  54.1 1.1 %combine.1 = bf16[256,512]{1,0:T(8,128)(2,1)} custom-call(bf16[1024,256]{1,0:T(8,128)(2,1)S(1)} %bitcast.10, bf16[2,256,1024]{2,1,0:T(8,128)(2,1)S(1)} %get-tuple-element.12.mix_ref), custom_call_target="tpu_custom_call" | custom-call | tf_op jit(solution)/shard_map/combine/pallas_call | solution.py:227
Async XLA Ops:
  0.0 29.9 %copy-start = (bf16[2,1024,1792]{2,1,0:T(8,128)(2,1)S(1)}, bf16[2,1024,1792]{2,1,0:T(8,128)(2,1)}, u32[]{:S(2)}) copy-start(bf16[2,1024,1792]{2,1,0:T(8,128)(2,1)} %wg_ref.3) | copy-start | bytes 22020100
  0.0 29.9 %copy-start.1 = (bf16[2,1024,1792]{2,1,0:T(8,128)(2,1)S(1)}, bf16[2,1024,1792]{2,1,0:T(8,128)(2,1)}, u32[]{:S(2)}) copy-start(bf16[2,1024,1792]{2,1,0:T(8,128)(2,1)} %wu_ref.3) | copy-start | bytes 22020100
  0.0 29.9 %copy-start.2 = (bf16[2,1792,1024]{2,1,0:T(8,128)(2,1)S(1)}, bf16[2,1792,1024]{2,1,0:T(8,128)(2,1)}, u32[]{:S(2)}) copy-start(bf16[2,1792,1024]{2,1,0:T(8,128)(2,1)} %wd_ref.3) | copy-start | bytes 22020100
  4.6 25.3 %collective-permute-start = (bf16[2,1024,1792]{2,1,0:T(8,128)(2,1)S(1)}, bf16[2,1024,1792]{2,1,0:T(8,128)(2,1)S(1)}, u32[]{:S(2)}, u32[]{:S(2)}) collective-permute-start(bf16[2,1024,1792]{2,1,0:T(8,128)(2,1)S(1)} %get-tuple-element.10), channel_id=1, source_target_pairs={{0,1},{1,0},{2,3},{3,2},{4,5},{5,4},{6,7},{7,6},{8,9},{9,8},{10,11... | collective-permute-start | bytes 22020104 | tf_op jit(solution)/shard_map/ppermute | solution.py:246
  6.1 23.8 %collective-permute-start.1 = (bf16[1792,1024]{1,0:T(8,128)(2,1)S(1)}, bf16[1792,1024]{1,0:T(8,128)(2,1)S(1)}, u32[]{:S(2)}, u32[]{:S(2)}) collective-permute-start(bf16[1792,1024]{1,0:T(8,128)(2,1)S(1)} %get-tuple-element.11), channel_id=1, source_target_pairs={{0,1},{1,0},{2,3},{3,2},{4,5},{5,4},{6,7},{7,6},{8,9},{9,8},{10,11... | collective-permute-start | bytes 11010056 | tf_op jit(solution)/shard_map/ppermute | solution.py:246

commit v4 on v3

--- a/solution.py
+++ b/solution.py
@@ -42,16 +42,26 @@
     return jnp.where(hit, before, -1.0)
 
 
-def fetch(pairs, sems):
+def fetch(pairs, sems, priority=0):
     copies = [pltpu.make_async_copy(src, dst, sems.at[i]) for i, (src, dst) in enumerate(pairs)]
     for copy in copies:
-        copy.start()
+        copy.start(priority=priority)
     return copies
+
+
+def folded(hidden, width):
+    rest = hidden - width
+    blocks = [((pl.ds(0, width), pl.ds(0, width)), (pl.ds(0, width), pl.ds(0, width)))]
+    blocks.append(((pl.ds(width, rest), pl.ds(0, rest)), (pl.ds(0, rest), pl.ds(width, rest))))
+    for i in range(rest // CHUNK):
+        rows = pl.ds(width + i * CHUNK, CHUNK)
+        blocks.append(((rows, pl.ds(rest, CHUNK)), (pl.ds(rest, CHUNK), rows)))
+    return blocks
 
 
 def prep_kernel(
     tok_hbm, gain_hbm, route_hbm, len_hbm, share_hbm, wg_ref, wu_ref, wd_ref,
-    out_ref, mix_ref, sgu_ref, sd_ref,
+    out_ref, mix_ref, swap_ref,
     tok_ref, gain_ref, route_ref, len_ref, share_ref, small_sems, sems,
 ):
     me = lax.axis_index("tp")
@@ -62,9 +72,9 @@
         ),
         small_sems,
     )
-    large = fetch(
-        ((wg_ref.at[1 - me], sgu_ref.at[0]), (wu_ref.at[1 - me], sgu_ref.at[1]), (wd_ref.at[1 - me], sd_ref)), sems
-    )
+    theirs = wd_ref.at[1 - me]
+    folds = [(theirs.at[here], swap_ref.at[2].at[there]) for here, there in folded(*theirs.shape)]
+    large = fetch([(wg_ref.at[1 - me], swap_ref.at[0]), (wu_ref.at[1 - me], swap_ref.at[1])] + folds, sems, 1)
     for copy in small[:2]:
         copy.wait()
     rows, width = tok_ref.shape
@@ -112,11 +122,10 @@
         out_shape=(
             jax.ShapeDtypeStruct((8 * chips, width // 2), bf16),
             pltpu.VMEM((2, rows, 16 * chips), bf16),
-            pltpu.VMEM((2, width, hidden), bf16),
-            pltpu.VMEM((hidden, width), bf16),
+            pltpu.VMEM((3, width, hidden), bf16),
         ),
         in_specs=[pl.BlockSpec(memory_space=pltpu.HBM)] * 8,
-        out_specs=(pl.BlockSpec(memory_space=pltpu.VMEM),) * 4,
+        out_specs=(pl.BlockSpec(memory_space=pltpu.VMEM),) * 3,
         scratch_shapes=[
             pltpu.VMEM(tokens.shape, bf16),
             pltpu.VMEM(gain.shape, f32),
@@ -124,15 +133,16 @@
             pltpu.VMEM(lengths.shape, jnp.int32),
             pltpu.VMEM(shares.shape, f32),
             pltpu.SemaphoreType.DMA((5,)),
-            pltpu.SemaphoreType.DMA((3,)),
+            pltpu.SemaphoreType.DMA((2 + len(folded(hidden, width)),)),
         ],
         compiler_params=pltpu.CompilerParams(vmem_limit_bytes=12 << 20),
     )(*in_hbm(tokens, gain, routes, lengths, shares, w_gate, w_up, w_down))
 
 
-def expert_kernel(in_ref, sgu_ref, sd_ref, wg_ref, wu_ref, wd_ref, out_ref, x_buf, y_buf, h_buf):
+def expert_kernel(in_ref, swap_ref, wg_ref, wu_ref, wd_ref, out_ref, x_buf, y_buf, h_buf):
     me = lax.axis_index("tp")
-    hidden, width = sd_ref.shape
+    _, width, hidden = swap_ref.shape
+    rest = hidden - width
     half = width // 2
     parts = hidden // CHUNK
     blocks = width // CHUNK
@@ -167,11 +177,18 @@
             h_buf[:rows, pl.ds(base + i * CHUNK, CHUNK)] = (gate / (1.0 + jnp.exp(-gate)) * up).astype(bf16)
 
     def run(rows):
-        hide(rows, sgu_ref.at[0], sgu_ref.at[1], 0)
+        hide(rows, swap_ref.at[0], swap_ref.at[1], 0)
         hide(rows, wg_ref.at[me], wu_ref.at[me], hidden)
         for i in range(blocks):
             cols = pl.ds(i * CHUNK, CHUNK)
-            total = dot(h_buf[:rows, :hidden], sd_ref[:, cols]) + dot(h_buf[:rows, hidden:], wd_ref[me, :, cols])
+            total = dot(h_buf[:rows, hidden:], wd_ref[me, :, cols])
+            total = total + dot(h_buf[:rows, :width], swap_ref[2, :, cols])
+            if i * CHUNK < rest:
+                total = total + dot(h_buf[:rows, width:hidden], swap_ref[2, :rest, pl.ds(width + i * CHUNK, CHUNK)])
+            else:
+                for j in range(rest // CHUNK):
+                    part = pl.ds(width + j * CHUNK, CHUNK)
+                    total = total + dot(h_buf[:rows, part], swap_ref[2, rest:, part])
             y_buf[:rows, cols] = total.astype(bf16)
         if rows < slots:
             y_buf[rows:] = jnp.zeros((slots - rows, width), bf16)
@@ -197,15 +214,15 @@
         out_ref[:, 1, core] = jnp.where(low, pltpu.roll(a, SLOTS, 1), b).astype(bf16)
 
 
-def expert(arrived, gate_up, down, w_gate, w_up, w_down):
-    hidden, width = down.shape
+def expert(arrived, swapped, w_gate, w_up, w_down):
+    _, width, hidden = swapped.shape
     rows = arrived.shape[0] // 2
     vmem = pl.BlockSpec(memory_space=pltpu.VMEM)
     return pl.pallas_call(
         expert_kernel,
         name="expert",
         out_shape=jax.ShapeDtypeStruct((rows // 8, 2, 2, 8, width // 4), bf16),
-        in_specs=[vmem] * 6,
+        in_specs=[vmem] * 5,
         out_specs=vmem,
         scratch_shapes=[
             pltpu.VMEM((rows, width), bf16),
@@ -213,7 +230,7 @@
             pltpu.VMEM((rows, 2 * hidden), bf16),
         ],
         compiler_params=pltpu.CompilerParams(vmem_limit_bytes=8 << 20),
-    )(arrived, gate_up, down, *[pltpu.with_memory_space_constraint(w, pltpu.VMEM) for w in (w_gate, w_up, w_down)])
+    )(arrived, swapped, *[pltpu.with_memory_space_constraint(w, pltpu.VMEM) for w in (w_gate, w_up, w_down)])
 
 
 def combine_kernel(in_ref, mix_ref, out_ref):
@@ -240,12 +257,12 @@
     routes = routing.T
     weights = route_weights.T
     spans = lengths.reshape(1, -1)
-    outgoing, mix, gate_up, down = prep(
+    outgoing, mix, others = prep(
         tokens, norm_gain.reshape(1, -1), routes, spans, weights, w_gate, w_up, w_down
     )
-    gate_up, down = (lax.ppermute(half, "tp", [(0, 1), (1, 0)]) for half in (gate_up, down))
+    swapped = lax.ppermute(others, "tp", [(0, 1), (1, 0)])
     arrived = lax.all_to_all(outgoing.reshape(chips, 8, width // 2), "ep", split_axis=0, concat_axis=0, tiled=True)
-    results = expert(arrived.reshape(chips * 8, width // 2), gate_up, down, w_gate, w_up, w_down)
+    results = expert(arrived.reshape(chips * 8, width // 2), swapped, w_gate, w_up, w_down)
     returned = lax.all_to_all(
         results.reshape(2 * chips, 8, width // 4), ("ep", "tp"), split_axis=0, concat_axis=0, tiled=True
     )

time: 55.3 us -> 55.1 us (level)
    ppermute x2 -> x1, starting transfers between devices: 1.55 us -> 1.45 us  [per_device(): swapped = lax.ppermute(others, 'tp', [(0, 1), (1, 0)])]
  transfers between devices with their start and end apart: 2 -> 1, of which waited for: 0 -> 0; matrix products, arithmetic and copies ran while one was open for 0% -> 0% of each run, Pallas kernels for 0% -> 0%
where the time goes in v4:
time: 55.1 us; the launch traced here: 55 us
  blocking collectives  42.3 us (77%)
  Pallas kernels  11.1 us (20%)
  starting transfers between devices  1.45 us (3%)
    all_to_all x1, blocking collectives, per_device(): lax.all_to_all(outgoing.reshape(chips, 8, width // 2), 'ep', split_axis=0...  24.1 us
    all_to_all x1, blocking collectives, per_device(): lax.all_to_all(results.reshape(2 * chips, 8, width // 4), ('ep', 'tp'), s...  18.3 us
    pallas_call x1, Pallas kernels, expert(): pl.pallas_call(expert_kernel, name='expert', out_shape=jax.ShapeDtypeStru...  5.48 us
    pallas_call x1, Pallas kernels, prep(): pl.pallas_call(prep_kernel, name='prep', out_shape=(jax.ShapeDtypeStruct(...  4.52 us
    ppermute x1, starting transfers between devices, per_device(): swapped = lax.ppermute(others, 'tp', [(0, 1), (1, 0)])  1.45 us
    pallas_call x1, Pallas kernels, combine(): pl.pallas_call(combine_kernel, name='combine', out_shape=jax.ShapeDtypeSt...  1.14 us
  transfers between devices with their start and end apart: 1, of which 0 were waited for; matrix products, arithmetic and copies ran while one was open for 0% of the time, Pallas kernels for 0%

profile of v4, /device:TPU:1, one launch (start us, length us, event | category | flops | bytes accessed | tf_op | source)
XLA Modules:
  0.0 55.0 jit_solution(16947736752285084925)
XLA Ops:
  0.0 0.0 copy-start
  0.0 0.0 copy-start.1
  0.0 0.0 copy-start.2
  0.0 4.5 %prep.1 = (bf16[512,512]{1,0:T(8,128)(2,1)S(1)}, bf16[2,256,1024]{2,1,0:T(8,128)(2,1)S(1)}, bf16[3,1024,1792]{2,1,0:T(8,128)(2,1)S(1)}) custom-call(bf16[256,1024]{1,0:T(8,128)(2,1)} %tok_hbm.1, f32[1,1024]{1,0:T(1,128)} %bitcast.12, s32[2,256]{1,0:T(2,128)} %bitcast.13, s32[1,64]{1,0:T(1,128)} %bitcast.15, f32[2,256]{1,0:T(2,128)} %bitcast.14, ...), custom_call_target="tpu_custom_call" | custom-call | tf_op jit(solution)/shard_map/prep/pallas_call | solution.py:119
  4.5 1.5 %collective-permute-start = (bf16[3,1024,1792]{2,1,0:T(8,128)(2,1)S(1)}, bf16[3,1024,1792]{2,1,0:T(8,128)(2,1)S(1)}, u32[]{:S(2)}, u32[]{:S(2)}) collective-permute-start(bf16[3,1024,1792]{2,1,0:T(8,128)(2,1)S(1)} %get-tuple-element.9), channel_id=1, source_target_pairs={{0,1},{1,0},{2,3},{3,2},{4,5},{5,4},{6,7},{7,6},{8,9},{9,8},{10,11... | collective-permute-start | bytes 33030152 | tf_op jit(solution)/shard_map/ppermute | solution.py:263
  6.0 24.1 %all_to_all.10 = bf16[64,8,512]{2,1,0:T(8,128)(2,1)S(1)} all-to-all(bf16[64,8,512]{2,1,0:T(8,128)(2,1)S(1)} %bitcast.11), channel_id=1, replica_groups=mesh['ep'=64,'tp'=2] {'ep'}, dimensions={0} | all-to-all | bytes 1048576 | tf_op jit(solution)/shard_map/all_to_all | solution.py:264
  30.1 0.0 collective-permute-done.swap_ref
  30.1 0.0 copy-done
  30.1 0.0 copy-done.1
  30.1 0.0 copy-done.2
  30.1 5.5 %expert.1 = bf16[32,2,2,8,256]{4,3,2,1,0:T(8,128)(2,1)S(1)} custom-call(bf16[512,512]{1,0:T(8,128)(2,1)S(1)} %bitcast.8, bf16[3,1024,1792]{2,1,0:T(8,128)(2,1)S(1)} %collective-permute-done.swap_ref, bf16[2,1024,1792]{2,1,0:T(8,128)(2,1)S(1)} %copy-done, bf16[2,1024,1792]{2,1,0:T(8,128)(2,1)S(1)} %copy-done.1, bf16[2,1792,1024]{2,1,0:T(8,128)(2,1)S(1)} %copy-done.2), custom_call_target="tpu_custom_call" | custom-call | tf_op jit(solution)/shard_map/expert/pallas_call | solution.py:221
  35.6 18.3 %all_to_all.11 = bf16[128,8,256]{2,1,0:T(8,128)(2,1)S(1)} all-to-all(bf16[128,8,256]{2,1,0:T(8,128)(2,1)S(1)} %bitcast.9), channel_id=1, replica_groups=mesh['ep'=64,'tp'=2] {'ep','tp'}, dimensions={0} | all-to-all | bytes 1048576 | tf_op jit(solution)/shard_map/all_to_all | solution.py:266
  53.8 1.1 %combine.1 = bf16[256,512]{1,0:T(8,128)(2,1)} custom-call(bf16[1024,256]{1,0:T(8,128)(2,1)S(1)} %bitcast.10, bf16[2,256,1024]{2,1,0:T(8,128)(2,1)S(1)} %get-tuple-element.10.mix_ref), custom_call_target="tpu_custom_call" | custom-call | tf_op jit(solution)/shard_map/combine/pallas_call | solution.py:244
Async XLA Ops:
  0.0 30.1 %copy-start = (bf16[2,1024,1792]{2,1,0:T(8,128)(2,1)S(1)}, bf16[2,1024,1792]{2,1,0:T(8,128)(2,1)}, u32[]{:S(2)}) copy-start(bf16[2,1024,1792]{2,1,0:T(8,128)(2,1)} %wg_ref.3) | copy-start | bytes 22020100
  0.0 30.1 %copy-start.1 = (bf16[2,1024,1792]{2,1,0:T(8,128)(2,1)S(1)}, bf16[2,1024,1792]{2,1,0:T(8,128)(2,1)}, u32[]{:S(2)}) copy-start(bf16[2,1024,1792]{2,1,0:T(8,128)(2,1)} %wu_ref.3) | copy-start | bytes 22020100
  0.0 30.1 %copy-start.2 = (bf16[2,1792,1024]{2,1,0:T(8,128)(2,1)S(1)}, bf16[2,1792,1024]{2,1,0:T(8,128)(2,1)}, u32[]{:S(2)}) copy-start(bf16[2,1792,1024]{2,1,0:T(8,128)(2,1)} %wd_ref.3) | copy-start | bytes 22020100
  4.5 25.5 %collective-permute-start = (bf16[3,1024,1792]{2,1,0:T(8,128)(2,1)S(1)}, bf16[3,1024,1792]{2,1,0:T(8,128)(2,1)S(1)}, u32[]{:S(2)}, u32[]{:S(2)}) collective-permute-start(bf16[3,1024,1792]{2,1,0:T(8,128)(2,1)S(1)} %get-tuple-element.9), channel_id=1, source_target_pairs={{0,1},{1,0},{2,3},{3,2},{4,5},{5,4},{6,7},{7,6},{8,9},{9,8},{10,11... | collective-permute-start | bytes 33030152 | tf_op jit(solution)/shard_map/ppermute | solution.py:263

commit v5 on v4

--- a/solution.py
+++ b/solution.py
@@ -148,15 +148,17 @@
     blocks = width // CHUNK
     pairs = in_ref.shape[0] // 16
     slots = 8 * pairs
-    arrived = in_ref[...].astype(f32).reshape(pairs, 2, 8, half)
-    even, odd = arrived[:, 0], arrived[:, 1]
-    low = iota((pairs, 8, half), 1) < SLOTS
-    first = jnp.where(low, even, pltpu.roll(odd, SLOTS, 1)).reshape(slots, half)
-    second = jnp.where(low, pltpu.roll(even, SLOTS, 1), odd).reshape(slots, half)
-    peak = jnp.zeros((slots, 128), f32)
+    low = iota((pairs, 8, 128), 1) < SLOTS
+    peak = jnp.zeros((pairs, 8, 128), f32)
     for i in range(half // 128):
-        lanes = slice(i * 128, (i + 1) * 128)
-        peak = jnp.maximum(peak, jnp.maximum(jnp.abs(first[:, lanes]), jnp.abs(second[:, lanes])))
+        arrived = in_ref[:, i * 128 : (i + 1) * 128].astype(f32).reshape(pairs, 2, 8, 128)
+        even, odd = arrived[:, 0], arrived[:, 1]
+        first = jnp.where(low, even, pltpu.roll(odd, SLOTS, 1))
+        second = jnp.where(low, pltpu.roll(even, SLOTS, 1), odd)
+        y_buf[:, i * 128 : (i + 1) * 128] = first.reshape(slots, 128).astype(bf16)
+        y_buf[:, half + i * 128 : half + (i + 1) * 128] = second.reshape(slots, 128).astype(bf16)
+        peak = jnp.maximum(peak, jnp.maximum(jnp.abs(first), jnp.abs(second)))
+    peak = peak.reshape(slots, 128)
     filled = lax.dot_general(
         jnp.ones((8, 128), bf16), (peak > 0.0).astype(bf16), (((1,), (1,)), ((), ())), preferred_element_type=f32
     )
@@ -165,8 +167,9 @@
     place = jnp.where(live, dot(live.astype(bf16), earlier), -1.0)
     amount = jnp.sum(live[0:1].astype(jnp.int32))
     squeeze = (iota((slots, slots), 0).astype(f32) == place[0:1]).astype(bf16)
-    x_buf[:, :half] = dot(squeeze, first.astype(bf16)).astype(bf16)
-    x_buf[:, half:] = dot(squeeze, second.astype(bf16)).astype(bf16)
+    for i in range(blocks):
+        cols = slice(i * CHUNK, (i + 1) * CHUNK)
+        x_buf[:, cols] = dot(squeeze, y_buf[:, cols]).astype(bf16)
 
     def hide(rows, gates, ups, base):
         x = x_buf[:rows]

time: 55.1 us -> 55.1 us (level)
  no operation moved by 1% of the time
where the time goes in v5:
time: 55.1 us; the launch traced here: 55 us
  blocking collectives  42.3 us (77%)
  Pallas kernels  11.2 us (20%)
  starting transfers between devices  1.45 us (3%)
    all_to_all x1, blocking collectives, per_device(): lax.all_to_all(outgoing.reshape(chips, 8, width // 2), 'ep', split_axis=0...  24.1 us
    all_to_all x1, blocking collectives, per_device(): lax.all_to_all(results.reshape(2 * chips, 8, width // 4), ('ep', 'tp'), s...  18.3 us
    pallas_call x1, Pallas kernels, expert(): pl.pallas_call(expert_kernel, name='expert', out_shape=jax.ShapeDtypeStru...  5.5 us
    pallas_call x1, Pallas kernels, prep(): pl.pallas_call(prep_kernel, name='prep', out_shape=(jax.ShapeDtypeStruct(...  4.52 us
    ppermute x1, starting transfers between devices, per_device(): swapped = lax.ppermute(others, 'tp', [(0, 1), (1, 0)])  1.45 us
    pallas_call x1, Pallas kernels, combine(): pl.pallas_call(combine_kernel, name='combine', out_shape=jax.ShapeDtypeSt...  1.14 us
  transfers between devices with their start and end apart: 1, of which 0 were waited for; matrix products, arithmetic and copies ran while one was open for 0% of the time, Pallas kernels for 0%

profile of v5, /device:TPU:1, one launch (start us, length us, event | category | flops | bytes accessed | tf_op | source)
XLA Modules:
  0.0 55.0 jit_solution(7818913669333087654)
XLA Ops:
  0.0 0.0 copy-start
  0.0 0.0 copy-start.1
  0.0 0.0 copy-start.2
  0.0 4.5 %prep.1 = (bf16[512,512]{1,0:T(8,128)(2,1)S(1)}, bf16[2,256,1024]{2,1,0:T(8,128)(2,1)S(1)}, bf16[3,1024,1792]{2,1,0:T(8,128)(2,1)S(1)}) custom-call(bf16[256,1024]{1,0:T(8,128)(2,1)} %tok_hbm.1, f32[1,1024]{1,0:T(1,128)} %bitcast.12, s32[2,256]{1,0:T(2,128)} %bitcast.13, s32[1,64]{1,0:T(1,128)} %bitcast.15, f32[2,256]{1,0:T(2,128)} %bitcast.14, ...), custom_call_target="tpu_custom_call" | custom-call | tf_op jit(solution)/shard_map/prep/pallas_call | solution.py:119
  4.5 1.5 %collective-permute-start = (bf16[3,1024,1792]{2,1,0:T(8,128)(2,1)S(1)}, bf16[3,1024,1792]{2,1,0:T(8,128)(2,1)S(1)}, u32[]{:S(2)}, u32[]{:S(2)}) collective-permute-start(bf16[3,1024,1792]{2,1,0:T(8,128)(2,1)S(1)} %get-tuple-element.9), channel_id=1, source_target_pairs={{0,1},{1,0},{2,3},{3,2},{4,5},{5,4},{6,7},{7,6},{8,9},{9,8},{10,11... | collective-permute-start | bytes 33030152 | tf_op jit(solution)/shard_map/ppermute | solution.py:266
  6.0 24.1 %all_to_all.10 = bf16[64,8,512]{2,1,0:T(8,128)(2,1)S(1)} all-to-all(bf16[64,8,512]{2,1,0:T(8,128)(2,1)S(1)} %bitcast.11), channel_id=1, replica_groups=mesh['ep'=64,'tp'=2] {'ep'}, dimensions={0} | all-to-all | bytes 1048576 | tf_op jit(solution)/shard_map/all_to_all | solution.py:267
  30.1 0.0 collective-permute-done.swap_ref
  30.1 0.0 copy-done
  30.1 0.0 copy-done.1
  30.1 0.0 copy-done.2
  30.1 5.5 %expert.1 = bf16[32,2,2,8,256]{4,3,2,1,0:T(8,128)(2,1)S(1)} custom-call(bf16[512,512]{1,0:T(8,128)(2,1)S(1)} %bitcast.8, bf16[3,1024,1792]{2,1,0:T(8,128)(2,1)S(1)} %collective-permute-done.swap_ref, bf16[2,1024,1792]{2,1,0:T(8,128)(2,1)S(1)} %copy-done, bf16[2,1024,1792]{2,1,0:T(8,128)(2,1)S(1)} %copy-done.1, bf16[2,1792,1024]{2,1,0:T(8,128)(2,1)S(1)} %copy-done.2), custom_call_target="tpu_custom_call" | custom-call | tf_op jit(solution)/shard_map/expert/pallas_call | solution.py:224
  35.6 18.3 %all_to_all.11 = bf16[128,8,256]{2,1,0:T(8,128)(2,1)S(1)} all-to-all(bf16[128,8,256]{2,1,0:T(8,128)(2,1)S(1)} %bitcast.9), channel_id=1, replica_groups=mesh['ep'=64,'tp'=2] {'ep','tp'}, dimensions={0} | all-to-all | bytes 1048576 | tf_op jit(solution)/shard_map/all_to_all | solution.py:269
  53.9 1.1 %combine.1 = bf16[256,512]{1,0:T(8,128)(2,1)} custom-call(bf16[1024,256]{1,0:T(8,128)(2,1)S(1)} %bitcast.10, bf16[2,256,1024]{2,1,0:T(8,128)(2,1)S(1)} %get-tuple-element.10.mix_ref), custom_call_target="tpu_custom_call" | custom-call | tf_op jit(solution)/shard_map/combine/pallas_call | solution.py:247
Async XLA Ops:
  0.0 30.1 %copy-start = (bf16[2,1024,1792]{2,1,0:T(8,128)(2,1)S(1)}, bf16[2,1024,1792]{2,1,0:T(8,128)(2,1)}, u32[]{:S(2)}) copy-start(bf16[2,1024,1792]{2,1,0:T(8,128)(2,1)} %wg_ref.3) | copy-start | bytes 22020100
  0.0 30.1 %copy-start.1 = (bf16[2,1024,1792]{2,1,0:T(8,128)(2,1)S(1)}, bf16[2,1024,1792]{2,1,0:T(8,128)(2,1)}, u32[]{:S(2)}) copy-start(bf16[2,1024,1792]{2,1,0:T(8,128)(2,1)} %wu_ref.3) | copy-start | bytes 22020100
  0.0 30.1 %copy-start.2 = (bf16[2,1792,1024]{2,1,0:T(8,128)(2,1)S(1)}, bf16[2,1792,1024]{2,1,0:T(8,128)(2,1)}, u32[]{:S(2)}) copy-start(bf16[2,1792,1024]{2,1,0:T(8,128)(2,1)} %wd_ref.3) | copy-start | bytes 22020100
  4.5 25.5 %collective-permute-start = (bf16[3,1024,1792]{2,1,0:T(8,128)(2,1)S(1)}, bf16[3,1024,1792]{2,1,0:T(8,128)(2,1)S(1)}, u32[]{:S(2)}, u32[]{:S(2)}) collective-permute-start(bf16[3,1024,1792]{2,1,0:T(8,128)(2,1)S(1)} %get-tuple-element.9), channel_id=1, source_target_pairs={{0,1},{1,0},{2,3},{3,2},{4,5},{5,4},{6,7},{7,6},{8,9},{9,8},{10,11... | collective-permute-start | bytes 33030152 | tf_op jit(solution)/shard_map/ppermute | solution.py:266
